TPU v7x, 32 devices: a whole 2x2x4 slice. The times are simulated.
32 devices in a mesh: grp: 2 (over y), fs: 4 (over z), tp: 4 (over x, core).
Axes of the slice: x: 2, y: 2, z: 4, core: 2. Of those that a mesh axis runs over, the one named last changes fastest.
Arguments:
- block_source_tensor: bfloat16 [4096, 2048], P(('grp', 'fs'), 'tp'), parts along dimension 0, may hold values from -6 to 6
- attend_initial_norm_gain: float32 [2048], replicated, may hold values from 0.1 to 1.9
- each_channel_group_norm: float32 [8, 256], P('tp'), may hold values from 0.1 to 1.9
- attend_final_norm_gain: float32 [2048], replicated, may hold values from 0.1 to 1.9
- dense_initial_norm_gain: float32 [2048], replicated, may hold values from 0.1 to 1.9
- dense_final_norm_gain: float32 [2048], replicated, may hold values from 0.1 to 1.9
- question_map: bfloat16 [2048, 1024], P('fs', 'tp'), may hold values from -0.125 to 0.125
- address_map: bfloat16 [2048, 1024], P('fs', 'tp'), may hold values from -0.125 to 0.125
- payload_weights_map: bfloat16 [2048, 2048], P('fs', 'tp'), may hold values from -0.125 to 0.125
- fading_left_factor: bfloat16 [2048, 16], replicated, may hold values from -0.125 to 0.125
- fading_right_factor: float32 [16, 1024], P(None, 'tp'), may hold values from -1.5 to 1.5
- fading_valve_constant: float32 [1024], P('tp'), may hold values from 0.05 to 6.2
- sudden_fade_excess: float32 [4096, 1024], P(('grp', 'fs'), 'tp'), parts along dimension 0, may hold values from -0.7 to 0
- combining_map: bfloat16 [2048, 2048], P('tp', 'fs')
- valve_map: bfloat16 [2048, 3072], P('fs', 'tp'), may hold values from -0.125 to 0.125
- widening_map: bfloat16 [2048, 3072], P('fs', 'tp'), may hold values from -0.125 to 0.125
- valve_conv_stencil: bfloat16 [3, 3072], P(None, 'tp'), may hold values from -3.5 to 3.5
- widening_conv_stencil: bfloat16 [3, 3072], P(None, 'tp'), may hold values from -3.5 to 3.5
- narrowing_map: bfloat16 [3072, 2048], P('tp', 'fs')
Outputs:
- layer_out: bfloat16 [4096, 2048], P(('grp', 'fs'), 'tp'), parts along dimension 0
There are 2 independent parts, one for each index of `grp`. A program takes and returns all parts, laid end to end along the dimension named above; an argument that names none is the same for every part. Nothing has to cross between parts.
All inputs are finite; a program needn't handle non-finite values.
Results may differ from a plain program's by a relative error of at most 0.019.
Values may be sent and summed in bfloat16 or wider, within the bound.
A program may use at most 128 MiB of HBM per device.

v0:
```python
import jax
import jax.numpy as jnp
from jax import lax
from jax.sharding import PartitionSpec as P

KEY_DIM = 128
VALUE_DIM = 256
BLOCK = 16


epsilon = 1e-06
valve_steepness = 16.0
careful_evaluation = lax.Precision.HIGHEST


def norm_rows(values, channel_gain):
    return (
        values
        * lax.rsqrt(jnp.mean(values * values, axis=-1, keepdims=True) + epsilon)
        * channel_gain
    )


def rounded(values):
    return lax.optimization_barrier(values.astype(jnp.bfloat16)).astype(jnp.float32)


def gated_linear(query_rows, key_rows, value_rows, fading_typical_span):
    length, head_count, key_width = query_rows.shape
    blocks = length // BLOCK
    query_rows = query_rows.reshape(blocks, BLOCK, head_count, key_width)
    key_rows = key_rows.reshape(blocks, BLOCK, head_count, key_width)
    value_rows = value_rows.reshape(blocks, BLOCK, head_count, -1)
    cumulative = jnp.cumsum(
        fading_typical_span.reshape(blocks, BLOCK, head_count, key_width), axis=1
    )
    tail_decay = cumulative[:, -1]
    query_in = query_rows * jnp.exp(cumulative)
    key_in = key_rows * jnp.exp(-cumulative)
    key_end = key_rows * jnp.exp(tail_decay[:, None] - cumulative)
    causal = jnp.tril(jnp.ones((BLOCK, BLOCK), dtype=bool))
    scores = jnp.einsum("nthk,nshk->nhts", query_in, key_in, precision=careful_evaluation)
    scores = jnp.where(causal, scores, 0.0)
    inner = jnp.einsum("nhts,nshv->nthv", scores, value_rows, precision=careful_evaluation)
    states = jnp.einsum("nshk,nshv->nhkv", key_end, value_rows, precision=careful_evaluation)

    def combine(earlier, latter):
        return (earlier[0] * latter[0], latter[0][..., None] * earlier[1] + latter[1])

    running = lax.associative_scan(combine, (jnp.exp(tail_decay), states))[1]
    carried = jnp.concatenate([jnp.zeros_like(running[:1]), running[:-1]], axis=0)
    outer = jnp.einsum("nthk,nhkv->nthv", query_in, carried, precision=careful_evaluation)
    return (inner + outer).reshape(length, head_count, -1)


def causal_taps(values, kernel):
    tap_count = kernel.shape[0]
    length = values.shape[0]
    padded = jnp.pad(values, ((tap_count - 1, 0), (0, 0)))
    kernel = kernel.astype(jnp.float32)
    summed = kernel[0] * padded[0:length]
    for offset in range(1, tap_count):
        summed = summed + kernel[offset] * padded[offset : offset + length]
    return summed


def add_products(pieces, normed):
    return tuple(
        (jnp.dot(normed, shard_rows, preferred_element_type=jnp.float32) for shard_rows in pieces)
    )


def on_device(
    block_source_tensor,
    attend_initial_norm_gain,
    each_channel_group_norm,
    attend_final_norm_gain,
    dense_initial_norm_gain,
    dense_final_norm_gain,
    question_map,
    address_map,
    payload_weights_map,
    fading_left_factor,
    fading_right_factor,
    fading_valve_constant,
    sudden_fade_excess,
    combining_map,
    valve_map,
    widening_map,
    valve_conv_stencil,
    widening_conv_stencil,
    narrowing_map,
):
    length, own_columns = block_source_tensor.shape
    tp_index = lax.axis_index("tp")
    full_width = own_columns * lax.axis_size("tp")
    full_rows = lax.all_gather(block_source_tensor, "tp", axis=1, tiled=True)
    normed = norm_rows(full_rows.astype(jnp.float32), attend_initial_norm_gain).astype(jnp.bfloat16)
    query_proj, key_proj, value_proj = add_products(
        (
            lax.all_gather(question_map, "fs", axis=0, tiled=True),
            lax.all_gather(address_map, "fs", axis=0, tiled=True),
            lax.all_gather(payload_weights_map, "fs", axis=0, tiled=True),
        ),
        normed,
    )
    head_count = each_channel_group_norm.shape[0]
    query_rows = rounded(query_proj).reshape(length, head_count, KEY_DIM) * KEY_DIM ** (-0.5)
    key_rows = rounded(key_proj).reshape(length, head_count, KEY_DIM)
    value_rows = rounded(value_proj).reshape(length, head_count, VALUE_DIM)
    fading_narrow_count = jnp.dot(normed, fading_left_factor, preferred_element_type=jnp.float32)
    fading_typical_span = (
        jax.nn.log_sigmoid(
            jnp.dot(fading_narrow_count, fading_right_factor, precision=careful_evaluation)
            + fading_valve_constant
        )
        / valve_steepness
        + sudden_fade_excess
    )
    mixed_heads = gated_linear(
        query_rows, key_rows, value_rows, fading_typical_span.reshape(length, head_count, KEY_DIM)
    )
    head_out = (
        norm_rows(mixed_heads, each_channel_group_norm)
        .astype(jnp.bfloat16)
        .reshape(length, head_count * VALUE_DIM)
    )
    partials = jnp.dot(
        head_out,
        lax.all_gather(combining_map, "fs", axis=1, tiled=True),
        preferred_element_type=jnp.float32,
    )
    mixed = lax.psum_scatter(
        partials.astype(jnp.bfloat16), "tp", scatter_dimension=1, tiled=True
    ).astype(jnp.float32)
    squares = lax.psum(jnp.sum(mixed * mixed, axis=1), "tp")
    own_gain = lax.dynamic_slice_in_dim(attend_final_norm_gain, tp_index * own_columns, own_columns)
    first = (
        block_source_tensor.astype(jnp.float32)
        + mixed * lax.rsqrt(squares / full_width + epsilon)[:, None] * own_gain
    ).astype(jnp.bfloat16)
    first_rows = lax.all_gather(first, "tp", axis=1, tiled=True)
    ffn_in = norm_rows(first_rows.astype(jnp.float32), dense_initial_norm_gain).astype(jnp.bfloat16)

    def add_single(shard_rows):
        return add_products((shard_rows,), ffn_in)[0]

    gate_pre = add_single(lax.all_gather(valve_map, "fs", axis=0, tiled=True))
    up_pre = add_single(lax.all_gather(widening_map, "fs", axis=0, tiled=True))
    hidden = (
        jax.nn.silu(causal_taps(gate_pre, valve_conv_stencil))
        * causal_taps(up_pre, widening_conv_stencil)
    ).astype(jnp.bfloat16)
    down_partials = jnp.dot(
        hidden,
        lax.all_gather(narrowing_map, "fs", axis=1, tiled=True),
        preferred_element_type=jnp.float32,
    )
    channel = lax.psum_scatter(
        down_partials.astype(jnp.bfloat16), "tp", scatter_dimension=1, tiled=True
    ).astype(jnp.float32)
    channel_squares = lax.psum(jnp.sum(channel * channel, axis=1), "tp")
    own_post = lax.dynamic_slice_in_dim(dense_final_norm_gain, tp_index * own_columns, own_columns)
    return (
        first.astype(jnp.float32)
        + channel * lax.rsqrt(channel_squares / full_width + epsilon)[:, None] * own_post
    ).astype(jnp.bfloat16)


def solution(mesh):
    placed = (
        P(("grp", "fs"), "tp"),
        P(),
        P("tp", None),
        P(),
        P(),
        P(),
        P("fs", "tp"),
        P("fs", "tp"),
        P("fs", "tp"),
        P(),
        P(None, "tp"),
        P("tp"),
        P(("grp", "fs"), "tp"),
        P("tp", "fs"),
        P("fs", "tp"),
        P("fs", "tp"),
        P(None, "tp"),
        P(None, "tp"),
        P("tp", "fs"),
    )
    return jax.shard_map(
        on_device, mesh=mesh, in_specs=placed, out_specs=P(("grp", "fs"), "tp"), check_vma=False
    )
```

profile of v0, /device:TPU:0, one launch (start us, length us, event | category | flops | bytes accessed | tf_op | source)
XLA Modules:
  0.0 574.9 jit_solution(4034378938816665195)
XLA Ops:
  11.1 23.1 %all-gather.10.cloned.1.call-done = bf16[512,2048]{1,0:T(8,128)(2,1)} async-done(((bf16[512,512]{1,0:T(8,128)(2,1)}), bf16[512,2048]{1,0:T(8,128)(2,1)}) %all-gather.10.cloned.1.call-update) | async-done | bytes 2097168 | tf_op jit(solution)/shard_map/all_gather | solution.py:97
  39.6 24.2 %all-gather.14.cloned.1.call-done = bf16[2048,256]{1,0:T(8,128)(2,1)} async-done(((bf16[512,256]{1,0:T(8,128)(2,1)}), bf16[2048,256]{1,0:T(8,128)(2,1)}) %all-gather.14.cloned.1.call-update) | async-done | bytes 1048592 | tf_op jit(solution)/shard_map/all_gather | solution.py:101
  66.1 26.6 %all-gather.16.cloned.1.call-done = bf16[2048,256]{1,0:T(8,128)(2,1)} async-done(((bf16[512,256]{1,0:T(8,128)(2,1)}), bf16[2048,256]{1,0:T(8,128)(2,1)}) %all-gather.16.cloned.1.call-update) | async-done | bytes 1048592 | tf_op jit(solution)/shard_map/all_gather | solution.py:102
  95.7 43.6 %all-gather.12.cloned.1.call-done = bf16[2048,512]{1,0:T(8,128)(2,1)} async-done(((bf16[512,512]{1,0:T(8,128)(2,1)}), bf16[2048,512]{1,0:T(8,128)(2,1)}) %all-gather.12.cloned.1.call-update) | async-done | bytes 2097168 | tf_op jit(solution)/shard_map/all_gather | solution.py:103
  163.0 4.0 pad.43
  173.8 11.6 %pad.45 = f32[16,2,128,256]{3,2,1,0:T(8,128)} pad(f32[8,2,128,256]{3,2,1,0:T(8,128)} %pad_maximum_fusion.1, f32[]{:T(128)} %constant.14.clone.1), padding=0_1_1x0_0_0x0_0_0x0_0_0 | pad | bytes 6291460 | tf_op jit(solution)/shard_map/pad | solution.py:50
  185.4 7.3 %pad.46 = f32[16,2,128,256]{3,2,1,0:T(8,128)} pad(f32[8,2,128,256]{3,2,1,0:T(8,128)S(1)} %copy-done.7, f32[]{:T(128)} %constant.14.clone.1), padding=1_0_1x0_0_0x0_0_0x0_0_0 | pad | bytes 6291460 | tf_op jit(solution)/shard_map/pad | solution.py:50
  192.7 6.2 %add.174 = f32[16,2,128,256]{3,2,1,0:T(8,128)} add(f32[16,2,128,256]{3,2,1,0:T(8,128)} %pad.45, f32[16,2,128,256]{3,2,1,0:T(8,128)} %pad.46) | non-fusion elementwise | flops 1048576 | bytes 12582912 | tf_op jit(solution)/shard_map/add | solution.py:50
  198.9 21.0 %pad.86 = f32[32,2,128,256]{3,2,1,0:T(8,128)} pad(f32[16,2,128,256]{3,2,1,0:T(8,128)} %add.174, f32[]{:T(128)} %constant.14.clone.1), padding=1_0_1x0_0_0x0_0_0x0_0_0 | pad | bytes 12582916
  219.9 5.1 fusion.8
  227.2 20.9 %pad.60 = f32[31,2,128,256]{3,2,1,0:T(8,128)} pad(f32[16,2,128,256]{3,2,1,0:T(8,128)} %pad_maximum_fusion, f32[]{:T(128)} %constant.14.clone.1), padding=0_0_1x0_0_0x0_0_0x0_0_0 | pad | bytes 12320772 | tf_op jit(solution)/shard_map/slice | solution.py:51
  248.2 8.3 %fusion = f32[32,2,256,16]{2,3,1,0:T(8,128)S(1)} fusion(f32[31,2,128,256]{3,2,1,0:T(8,128)} %pad.60, f32[32,16,2,128]{3,0,1,2:T(8,128)S(1)} %copy-done.9, f32[32,2,128,256]{3,2,1,0:T(8,128)} %pad.86), kind=kOutput, calls=%fused_computation | convolution fusion | flops 392101888 | bytes 17825792 | tf_op jit(solution)/shard_map/nthk,nhkv->nthv/dot_general | solution.py:52
  260.9 4.2 convolution_convert_fusion.1
  266.0 29.2 %reduce-scatter.3.cloned.1.call-done = bf16[512,512]{1,0:T(8,128)(2,1)} async-done(((bf16[512,2048]{1,0:T(8,128)(2,1)}), bf16[512,512]{1,0:T(8,128)(2,1)}) %reduce-scatter.3.cloned.1.call-update) | async-done | bytes 524304 | tf_op jit(solution)/shard_map/reduce_scatter | solution.py:133
  296.5 5.8 %psum.14 = f32[512]{0:T(512)S(1)} all-reduce(f32[512]{0:T(512)S(1)} %fusion.12), channel_id=1, replica_groups=mesh['grp'=2,'fs'=4,'tp'=4] {'tp'}, use_global_device_ids=true, to_apply=%region_5.6 | all-reduce | flops 512 | bytes 4096 | tf_op jit(solution)/shard_map/psum | solution.py:136
  306.9 20.8 %all-gather.20.cloned.1.call-done = bf16[512,2048]{1,0:T(8,128)(2,1)} async-done(((bf16[512,512]{1,0:T(8,128)(2,1)}), bf16[512,2048]{1,0:T(8,128)(2,1)}) %all-gather.20.cloned.1.call-update) | async-done | bytes 2097168 | tf_op jit(solution)/shard_map/all_gather | solution.py:142
  330.0 62.8 %all-gather.22.cloned.1.call-done = bf16[2048,768]{1,0:T(8,128)(2,1)} async-done(((bf16[512,768]{1,0:T(8,128)(2,1)}), bf16[2048,768]{1,0:T(8,128)(2,1)}) %all-gather.22.cloned.1.call-update) | async-done | bytes 3145744 | tf_op jit(solution)/shard_map/all_gather | solution.py:148
  392.8 4.9 fusion.30
  397.7 58.8 %all-gather.24.cloned.1.call-done = bf16[2048,768]{1,0:T(8,128)(2,1)} async-done(((bf16[512,768]{1,0:T(8,128)(2,1)}), bf16[2048,768]{1,0:T(8,128)(2,1)}) %all-gather.24.cloned.1.call-update) | async-done | bytes 3145744 | tf_op jit(solution)/shard_map/all_gather | solution.py:149
  456.5 4.9 fusion.28
  461.3 58.7 %all-gather.26.cloned.1.call-done = bf16[768,2048]{1,0:T(8,128)(2,1)} async-done(((bf16[768,512]{1,0:T(8,128)(2,1)}), bf16[768,2048]{1,0:T(8,128)(2,1)}) %all-gather.26.cloned.1.call-update) | async-done | bytes 3145744 | tf_op jit(solution)/shard_map/all_gather | solution.py:156
  520.0 9.3 %convolution_convert_fusion = bf16[512,2048]{1,0:T(8,128)(2,1)} fusion(bf16[768,2048]{1,0:T(8,128)(2,1)} %all-gather.26.cloned.1.call-done, f32[512,768]{1,0:T(8,128)} %fusion.28, f32[512,768]{1,0:T(8,128)} %fusion.30, f32[768]{0:T(1024)S(1)} %get-tuple-element.9, f32[768]{0:T(1024)S(1)} %get-tuple-element.10, f32[768]{0:T(1024)S(1)} %get-tuple-element.8, ...), kind=kOutput, calls=%fused_computation.16 | convolution fusion | flops 1617952768 | bytes 8407040 | tf_op jit(solution)/shard_map/dot_general | solution.py:154
  530.1 29.1 %reduce-scatter.5.cloned.1.call-done = bf16[512,512]{1,0:T(8,128)(2,1)} async-done(((bf16[512,2048]{1,0:T(8,128)(2,1)}), bf16[512,512]{1,0:T(8,128)(2,1)}) %reduce-scatter.5.cloned.1.call-update) | async-done | bytes 524304 | tf_op jit(solution)/shard_map/reduce_scatter | solution.py:159
  560.5 5.8 %psum.15 = f32[512]{0:T(512)S(1)} all-reduce(f32[512]{0:T(512)S(1)} %fusion.16), channel_id=1, replica_groups=mesh['grp'=2,'fs'=4,'tp'=4] {'tp'}, use_global_device_ids=true, to_apply=%region_9.10 | all-reduce | flops 512 | bytes 4096 | tf_op jit(solution)/shard_map/psum | solution.py:162
  (165 shorter events, 64.7 us)
Async XLA Ops:
  6.5 30.0 %copy-start = (bf16[2048,16]{0,1:T(8,128)(2,1)S(1)}, bf16[2048,16]{0,1:T(8,128)(2,1)}, u32[]{:S(2)}) copy-start(bf16[2048,16]{0,1:T(8,128)(2,1)} %param.28) | copy-start | bytes 196612
  6.5 30.0 %copy-start.24 = (f32[2048]{0:T(1024)S(1)}, f32[2048]{0:T(1024)}, u32[]{:S(2)}) copy-start(f32[2048]{0:T(1024)} %param.20) | copy-start | bytes 24580
  6.5 27.7 %all-gather.10.cloned.1.call-start = ((), (), s32[]{:S(2)}) async-start(), calls=%async_computation.2 | async-start | bytes 2621440 | tf_op jit(solution)/shard_map/all_gather | solution.py:97
  7.3 56.5 %all-gather.14.cloned.1.call-start = ((), (), s32[]{:S(2)}) async-start(), calls=%async_computation.4 | async-start | bytes 1310720 | tf_op jit(solution)/shard_map/all_gather | solution.py:101
  8.0 84.8 %all-gather.16.cloned.1.call-start = ((), (), s32[]{:S(2)}) async-start(), calls=%async_computation.5 | async-start | bytes 1310720 | tf_op jit(solution)/shard_map/all_gather | solution.py:102
  8.7 130.5 %all-gather.12.cloned.1.call-start = ((), (), s32[]{:S(2)}) async-start(), calls=%async_computation.3 | async-start | bytes 2621440 | tf_op jit(solution)/shard_map/all_gather | solution.py:103
  9.3 251.6 %all-gather.18.cloned.1.call-start = ((), (), s32[]{:S(2)}) async-start(), calls=%async_computation.6 | async-start | bytes 2621440 | tf_op jit(solution)/shard_map/all_gather | solution.py:130
  9.9 285.3 %reduce-scatter.3.cloned.1.call-start = ((), (), s32[]{:S(2)}) async-start(), calls=%async_computation.7 | async-start | bytes 2621440 | tf_op jit(solution)/shard_map/reduce_scatter | solution.py:133
  142.9 5.2 copy-start.10
  173.8 11.6 %copy-start.7 = (f32[8,2,128,256]{3,2,1,0:T(8,128)S(1)}, f32[8,2,128,256]{3,2,1,0:T(8,128)}, u32[]{:S(2)}) copy-start(f32[8,2,128,256]{3,2,1,0:T(8,128)} %add.172) | copy-start | bytes 6291460
  227.2 20.9 %copy-start.9 = (f32[32,16,2,128]{3,0,1,2:T(8,128)S(1)}, f32[32,16,2,128]{3,0,1,2:T(8,128)}, u32[]{:S(2)}) copy-start(f32[32,16,2,128]{3,0,1,2:T(8,128)} %get-tuple-element.15) | copy-start | bytes 1572868
  248.2 8.4 %copy-start.14 = (f32[32,16,2,128]{3,0,1,2:T(8,128)S(1)}, f32[32,16,2,128]{3,0,1,2:T(8,128)}, u32[]{:S(2)}) copy-start(f32[32,16,2,128]{3,0,1,2:T(8,128)} %get-tuple-element.11) | copy-start | bytes 1572868
  248.2 8.4 %copy-start.17 = (pred[16,16]{1,0:T(8,128)(4,1)S(1)}, pred[16,16]{1,0:T(8,128)(4,1)}, u32[]{:S(2)}) copy-start(pred[16,16]{1,0:T(8,128)(4,1)} %iota_compare_fusion) | copy-start | bytes 772
  248.2 10.0 %copy-start.11 = (bf16[32,16,2,256]{3,2,1,0:T(2,128)(2,1)S(1)}, bf16[32,16,2,256]{3,2,1,0:T(2,128)(2,1)}, u32[]{:S(2)}) copy-start(bf16[32,16,2,256]{3,2,1,0:T(2,128)(2,1)} %copy-done.10) | copy-start | bytes 1572868
  265.1 37.1 %copy-start.13 = (bf16[512,512]{1,0:T(8,128)(2,1)S(1)}, bf16[512,512]{1,0:T(8,128)(2,1)}, u32[]{:S(2)}) copy-start(bf16[512,512]{1,0:T(8,128)(2,1)} %param.19) | copy-start | bytes 1572868
  265.1 62.6 %all-gather.20.cloned.1.call-start = ((), (), s32[]{:S(2)}) async-start(), calls=%async_computation.8 | async-start | bytes 2621440 | tf_op jit(solution)/shard_map/all_gather | solution.py:142
  304.4 88.4 %copy-start.25 = (f32[2048]{0:T(1024)S(1)}, f32[2048]{0:T(1024)}, u32[]{:S(2)}) copy-start(f32[2048]{0:T(1024)} %param.23) | copy-start | bytes 24580
  304.4 88.4 %all-gather.22.cloned.1.call-start = ((), (), s32[]{:S(2)}) async-start(), calls=%async_computation.9 | async-start | bytes 3932160 | tf_op jit(solution)/shard_map/all_gather | solution.py:148
  305.1 151.3 %all-gather.24.cloned.1.call-start = ((), (), s32[]{:S(2)}) async-start(), calls=%async_computation.10 | async-start | bytes 3932160 | tf_op jit(solution)/shard_map/all_gather | solution.py:149
  305.9 214.1 %all-gather.26.cloned.1.call-start = ((), (), s32[]{:S(2)}) async-start(), calls=%async_computation.11 | async-start | bytes 3932160 | tf_op jit(solution)/shard_map/all_gather | solution.py:156
  306.5 252.8 %reduce-scatter.5.cloned.1.call-start = ((), (), s32[]{:S(2)}) async-start(), calls=%async_computation.12 | async-start | bytes 2621440 | tf_op jit(solution)/shard_map/reduce_scatter | solution.py:159
  327.7 65.0 %copy-start.16 = (bf16[512,2048]{1,0:T(8,128)(2,1)S(1)}, bf16[512,2048]{1,0:T(8,128)(2,1)}, u32[]{:S(2)}) copy-start(bf16[512,2048]{1,0:T(8,128)(2,1)} %all-gather.20.cloned.1.call-done) | copy-start | bytes 6291460
  529.3 37.0 %copy-start.12 = (bf16[512,512]{1,0:T(8,128)(2,1)S(1)}, bf16[512,512]{1,0:T(8,128)(2,1)}, u32[]{:S(2)}) copy-start(bf16[512,512]{1,0:T(8,128)(2,1)} %fusion.15) | copy-start | bytes 1572868
  529.3 39.1 %copy-start.1 = (bf16[2048,16]{0,1:T(8,128)(2,1)S(1)}, bf16[2048,16]{0,1:T(8,128)(2,1)}, u32[]{:S(2)}) copy-start(bf16[2048,16]{0,1:T(8,128)(2,1)} %param.28) | copy-start | bytes 196612
  (17 other events, 42.4 us)
Sparse Core Ops, SparseCore 0:
  8.9 25.2 all-gather.9
  35.8 27.9 all-gather.13
  65.4 27.3 all-gather.15
  94.2 45.0 all-gather.11
  140.7 44.4 all-gather.17
  265.3 29.9 reduce-scatter.2
  304.5 23.1 all-gather.19
  329.3 63.4 all-gather.21
  394.3 62.0 all-gather.23
  457.9 62.0 all-gather.25
  529.4 29.7 reduce-scatter.4
where the time goes:
time: 577 us; the launch traced here: 575 us
  waiting for transfers between devices  382 us (66%)
  local copies, waits for them, and re-layouts  81.9 us (14%)
  matrix products  47.2 us (8%)
  other arithmetic  37.6 us (7%)
  between operations  13.9 us (2%)
  blocking collectives  11.5 us (2%)
    all_gather x1, waiting for transfers between devices, on_device(): gate_pre = add_single(lax.all_gather(valve_map, 'fs', axis=0, tiled=True))  62.8 us
    all_gather x1, waiting for transfers between devices, on_device(): up_pre = add_single(lax.all_gather(widening_map, 'fs', axis=0, tiled=True))  58.8 us
    all_gather x1, waiting for transfers between devices, on_device(): lax.all_gather(narrowing_map, 'fs', axis=1, tiled=True)  58.7 us
    all_gather x1, waiting for transfers between devices, on_device(): lax.all_gather(payload_weights_map, 'fs', axis=0, tiled=True)  43.6 us
    reduce_scatter x1, waiting for transfers between devices, on_device(): lax.psum_scatter(partials.astype(jnp.bfloat16), 'tp', scatter_dimension=1...  29.2 us
    reduce_scatter x1, waiting for transfers between devices, on_device(): lax.psum_scatter(down_partials.astype(jnp.bfloat16), 'tp', scatter_dimens...  29.1 us
    unnamed x58, local copies, waits for them, and re-layouts  28.9 us
    pad x6, local copies, waits for them, and re-layouts, gated_linear(): running = lax.associative_scan(combine, (jnp.exp(tail_decay), states))[1]  27.1 us
  transfers between devices with their start and end apart: 11, of which 10 were waited for; matrix products, arithmetic and copies ran while one was open for 24% of the time, Pallas kernels for 0%

commit v1 on v0

v1 whole, which is shorter than its diff:
```python
import jax
import jax.numpy as jnp
from jax import lax
from jax.experimental import pallas as pl
from jax.experimental.pallas import tpu as pltpu
from jax.sharding import PartitionSpec as P

KEY_DIM = 128
VALUE_DIM = 256
BLOCK = 16


epsilon = 1e-06
valve_steepness = 16.0
careful_evaluation = lax.Precision.HIGHEST


def norm_rows(values, channel_gain):
    return (
        values
        * lax.rsqrt(jnp.mean(values * values, axis=-1, keepdims=True) + epsilon)
        * channel_gain
    )


CHUNK = 64


def contract(left, right, left_dim, right_dim):
    return lax.dot_general(
        left.astype(jnp.bfloat16),
        right.astype(jnp.bfloat16),
        (((left_dim,), (right_dim,)), ((), ())),
        preferred_element_type=jnp.float32,
    )


def mixing_kernel(q_ref, k_ref, v_ref, low_ref, right_ref, valve_ref, excess_ref, gain_ref, out_ref):
    length = q_ref.shape[0]
    head_count = gain_ref.shape[0]
    rows = lax.broadcasted_iota(jnp.int32, (CHUNK, CHUNK), 0)
    columns = lax.broadcasted_iota(jnp.int32, (CHUNK, CHUNK), 1)
    lower = (columns <= rows).astype(jnp.float32)

    def one_chunk(index, states):
        span = pl.ds(pl.multiple_of(index * CHUNK, CHUNK), CHUNK)
        logits = (
            jnp.dot(
                low_ref[span, :],
                right_ref[...],
                precision=careful_evaluation,
                preferred_element_type=jnp.float32,
            )
            + valve_ref[...]
        )
        fading = (
            jnp.minimum(logits, 0.0) - jnp.log1p(jnp.exp(-jnp.abs(logits)))
        ) / valve_steepness + excess_ref[span, :]
        total = jnp.dot(
            lower, fading, precision=careful_evaluation, preferred_element_type=jnp.float32
        )
        after = []
        for head in range(head_count):
            key_span = slice(head * KEY_DIM, (head + 1) * KEY_DIM)
            value_span = slice(head * VALUE_DIM, (head + 1) * VALUE_DIM)
            cum = total[:, key_span]
            query = q_ref[span, key_span].astype(jnp.float32) * KEY_DIM ** (-0.5)
            key = k_ref[span, key_span].astype(jnp.float32)
            value = v_ref[span, value_span]
            state = states[head]
            pieces = []
            for block in range(CHUNK // BLOCK):
                low, high = block * BLOCK, (block + 1) * BLOCK
                start = cum[low - 1 : low] if block else jnp.zeros((1, KEY_DIM), jnp.float32)
                query_in = query[low:high] * jnp.exp(cum[low:high] - start)
                key_in = jnp.concatenate(
                    [key[:high] * jnp.exp(start - cum[:high])]
                    + ([jnp.zeros((CHUNK - high, KEY_DIM), jnp.float32)] if high < CHUNK else []),
                    axis=0,
                )
                pieces.append(contract(query_in, key_in, 1, 1))
            scores = jnp.where(columns <= rows, jnp.concatenate(pieces, axis=0), 0.0)
            tail = cum[CHUNK - 1 :]
            mixed = contract(scores, value, 1, 0) + contract(query * jnp.exp(cum), state, 1, 1)
            after.append(state * jnp.exp(tail) + contract(value, key * jnp.exp(tail - cum), 0, 0))
            out_ref[span, value_span] = norm_rows(mixed, gain_ref[head : head + 1, :]).astype(
                jnp.bfloat16
            )
        return tuple(after)

    empty = tuple(jnp.zeros((VALUE_DIM, KEY_DIM), jnp.float32) for _ in range(head_count))
    lax.fori_loop(0, length // CHUNK, one_chunk, empty, unroll=2)


def mixing(query, key, value, low, right, valve, excess, gain):
    length = query.shape[0]
    flops = length * value.shape[1] * 8 * KEY_DIM
    return pl.pallas_call(
        mixing_kernel,
        out_shape=jax.ShapeDtypeStruct(value.shape, jnp.bfloat16),
        in_specs=[pl.BlockSpec(memory_space=pltpu.VMEM)] * 8,
        out_specs=pl.BlockSpec(memory_space=pltpu.VMEM),
        cost_estimate=pl.CostEstimate(
            flops=60 * flops, bytes_accessed=8 * value.size, transcendentals=0
        ),
    )(query, key, value, low, right, valve, excess, gain)


def causal_taps(values, kernel):
    tap_count = kernel.shape[0]
    length = values.shape[0]
    padded = jnp.pad(values, ((tap_count - 1, 0), (0, 0)))
    kernel = kernel.astype(jnp.float32)
    summed = kernel[0] * padded[0:length]
    for offset in range(1, tap_count):
        summed = summed + kernel[offset] * padded[offset : offset + length]
    return summed


def gather_parts(shard, dimension):
    copies = lax.axis_size("grp")
    part = shard.shape[dimension] // copies
    own = lax.dynamic_slice_in_dim(shard, lax.axis_index("grp") * part, part, axis=dimension)
    return lax.all_gather(own, ("fs", "grp"), axis=dimension, tiled=True)


def on_device(
    block_source_tensor,
    attend_initial_norm_gain,
    each_channel_group_norm,
    attend_final_norm_gain,
    dense_initial_norm_gain,
    dense_final_norm_gain,
    question_map,
    address_map,
    payload_weights_map,
    fading_left_factor,
    fading_right_factor,
    fading_valve_constant,
    sudden_fade_excess,
    combining_map,
    valve_map,
    widening_map,
    valve_conv_stencil,
    widening_conv_stencil,
    narrowing_map,
):
    length, own_columns = block_source_tensor.shape
    tp_index = lax.axis_index("tp")
    full_width = own_columns * lax.axis_size("tp")
    full_rows = lax.all_gather(block_source_tensor, "tp", axis=1, tiled=True)
    normed = norm_rows(full_rows.astype(jnp.float32), attend_initial_norm_gain).astype(jnp.bfloat16)
    qkv_map = gather_parts(
        jnp.concatenate([question_map, address_map, payload_weights_map], axis=1), 0
    )
    qk_columns = question_map.shape[1]
    projected = jnp.dot(normed, qkv_map, preferred_element_type=jnp.float32).astype(jnp.bfloat16)
    low_rank = jnp.dot(normed, fading_left_factor, preferred_element_type=jnp.float32)
    head_out = mixing(
        projected[:, :qk_columns],
        projected[:, qk_columns : 2 * qk_columns],
        projected[:, 2 * qk_columns :],
        low_rank,
        fading_right_factor,
        fading_valve_constant[None],
        sudden_fade_excess,
        each_channel_group_norm,
    )
    partials = jnp.dot(
        head_out,
        gather_parts(combining_map, 1),
        preferred_element_type=jnp.float32,
    )
    mixed = lax.psum_scatter(
        partials.astype(jnp.bfloat16), "tp", scatter_dimension=1, tiled=True
    ).astype(jnp.float32)
    squares = lax.psum(jnp.sum(mixed * mixed, axis=1), "tp")
    own_gain = lax.dynamic_slice_in_dim(attend_final_norm_gain, tp_index * own_columns, own_columns)
    first = (
        block_source_tensor.astype(jnp.float32)
        + mixed * lax.rsqrt(squares / full_width + epsilon)[:, None] * own_gain
    ).astype(jnp.bfloat16)
    first_rows = lax.all_gather(first, "tp", axis=1, tiled=True)
    ffn_in = norm_rows(first_rows.astype(jnp.float32), dense_initial_norm_gain).astype(jnp.bfloat16)

    gate_up_map = gather_parts(jnp.concatenate([valve_map, widening_map], axis=1), 0)
    units = valve_map.shape[1]
    gate_up = jnp.dot(ffn_in, gate_up_map, preferred_element_type=jnp.float32)
    gate_pre, up_pre = gate_up[:, :units], gate_up[:, units:]
    hidden = (
        jax.nn.silu(causal_taps(gate_pre, valve_conv_stencil))
        * causal_taps(up_pre, widening_conv_stencil)
    ).astype(jnp.bfloat16)
    down_partials = jnp.dot(
        hidden,
        gather_parts(narrowing_map, 1),
        preferred_element_type=jnp.float32,
    )
    channel = lax.psum_scatter(
        down_partials.astype(jnp.bfloat16), "tp", scatter_dimension=1, tiled=True
    ).astype(jnp.float32)
    channel_squares = lax.psum(jnp.sum(channel * channel, axis=1), "tp")
    own_post = lax.dynamic_slice_in_dim(dense_final_norm_gain, tp_index * own_columns, own_columns)
    return (
        first.astype(jnp.float32)
        + channel * lax.rsqrt(channel_squares / full_width + epsilon)[:, None] * own_post
    ).astype(jnp.bfloat16)


def solution(mesh):
    placed = (
        P(("grp", "fs"), "tp"),
        P(),
        P("tp", None),
        P(),
        P(),
        P(),
        P("fs", "tp"),
        P("fs", "tp"),
        P("fs", "tp"),
        P(),
        P(None, "tp"),
        P("tp"),
        P(("grp", "fs"), "tp"),
        P("tp", "fs"),
        P("fs", "tp"),
        P("fs", "tp"),
        P(None, "tp"),
        P(None, "tp"),
        P("tp", "fs"),
    )
    return jax.shard_map(
        on_device, mesh=mesh, in_specs=placed, out_specs=P(("grp", "fs"), "tp"), check_vma=False
    )
```

time: 577 us -> 444 us (0.77)
  local copies, waits for them, and re-layouts: 81.9 us -> 6.37 us
  matrix products: 47.2 us -> 23.5 us
  other arithmetic: 37.6 us -> 14 us
  waiting for transfers between devices: 382 us -> 365 us
  Pallas kernels: 0 us -> 8.75 us
    unnamed x58 -> x26, local copies, waits for them, and re-layouts: 28.9 us -> 0.05 us
    pad x6 -> x0, local copies, waits for them, and re-layouts: 27.1 us -> none  [gated_linear(): running = lax.associative_scan(combine, (jnp.exp(tail_decay), states))[1]]
    dot_general x12 -> x4, matrix products: 46.5 us -> 22.1 us  [the longest x1 7.52 us: on_device(): jnp.dot(hidden, gather_parts(narrowing_map, 1), preferred_element_type=jn...]
    add x12 -> x0, other arithmetic: 19.6 us -> none  [the longest x4 10.7 us: gated_linear(): running = lax.associative_scan(combine, (jnp.exp(tail_decay), states))[1]]
    slice x26 -> x3, local copies, waits for them, and re-layouts: 21.5 us -> 3.03 us  [the longest x1 1.35 us: on_device(): gate_pre, up_pre = (gate_up[:, :units], gate_up[:, units:])]
    all_gather x7 -> x4, waiting for transfers between devices: 275 us -> 262 us  [gather_parts(): return lax.all_gather(own, ('fs', 'grp'), axis=dimension, tiled=True)]
    pallas_call x0 -> x1, Pallas kernels: none -> 8.75 us  [mixing(): pl.pallas_call(mixing_kernel, out_shape=jax.ShapeDtypeStruct(value.shape,...]
  transfers between devices with their start and end apart: 11 -> 8, of which waited for: 10 -> 8; matrix products, arithmetic and copies ran while one was open for 24% -> 6% of each run, Pallas kernels for 0% -> 2%
where the time goes in v1:
time: 444 us; the launch traced here: 443 us
  waiting for transfers between devices  365 us (82%)
  matrix products  23.5 us (5%)
  other arithmetic  14 us (3%)
  between operations  13.7 us (3%)
  blocking collectives  11.5 us (3%)
  Pallas kernels  8.75 us (2%)
  local copies, waits for them, and re-layouts  6.37 us (1%)
    all_gather x4, waiting for transfers between devices, gather_parts(): return lax.all_gather(own, ('fs', 'grp'), axis=dimension, tiled=True)  262 us
    reduce_scatter x1, waiting for transfers between devices, on_device(): lax.psum_scatter(down_partials.astype(jnp.bfloat16), 'tp', scatter_dimens...  28.7 us
    reduce_scatter x1, waiting for transfers between devices, on_device(): lax.psum_scatter(partials.astype(jnp.bfloat16), 'tp', scatter_dimension=1...  28.5 us
    all_gather x1, waiting for transfers between devices, on_device(): full_rows = lax.all_gather(block_source_tensor, 'tp', axis=1, tiled=True)  24.1 us
    all_gather x1, waiting for transfers between devices, on_device(): first_rows = lax.all_gather(first, 'tp', axis=1, tiled=True)  21.3 us
  transfers between devices with their start and end apart: 8, of which 8 were waited for; matrix products, arithmetic and copies ran while one was open for 6% of the time, Pallas kernels for 2%

profile of v1, /device:TPU:0, one launch (start us, length us, event | category | flops | bytes accessed | tf_op | source)
XLA Modules:
  0.0 443.1 jit_solution(7009208565860667714)
XLA Ops:
  7.3 1.9 fusion.30
  10.1 24.1 %all-gather.7.cloned.1.call-done = bf16[512,2048]{1,0:T(8,128)(2,1)} async-done(((bf16[512,512]{1,0:T(8,128)(2,1)}), bf16[512,2048]{1,0:T(8,128)(2,1)}) %all-gather.7.cloned.1.call-update) | async-done | bytes 2097168 | tf_op jit(solution)/shard_map/all_gather | solution.py:151
  34.2 2.2 fusion
  36.5 1.5 fusion.26.low_ref
  38.0 71.2 %all-gather.9.cloned.1.call-done = bf16[2048,1024]{1,0:T(8,128)(2,1)} async-done(((bf16[256,1024]{1,0:T(8,128)(2,1)}), bf16[2048,1024]{1,0:T(8,128)(2,1)}) %all-gather.9.cloned.1.call-update) | async-done | bytes 4194320 | tf_op jit(solution)/shard_map/all_gather | solution.py:124
  109.2 4.6 %convolution_convert_fusion.2 = bf16[512,1024]{1,0:T(8,128)(2,1)S(1)} fusion(bf16[2048,1024]{1,0:T(8,128)(2,1)} %all-gather.9.cloned.1.call-done, bf16[512,2048]{1,0:T(8,128)(2,1)S(1)} %copy-done.3, f32[2048]{0:T(1024)S(1)} %copy-done.11, f32[512]{0:T(512)S(1)} %add_rsqrt_fusion.3), kind=kOutput, calls=%fused_computation.18 | convolution fusion | flops 2152202240 | bytes 7350272 | tf_op jit(solution)/shard_map/dot_general | solution.py:157
  115.4 8.7 %shard_map.181 = bf16[512,512]{1,0:T(8,128)(2,1)} custom-call(bf16[512,256]{1,0:T(8,128)(2,1)} %get-tuple-element.14.q_ref, bf16[512,256]{1,0:T(8,128)(2,1)} %get-tuple-element.13.k_ref, bf16[512,512]{1,0:T(8,128)(2,1)} %slice.64.v_ref, f32[512,16]{1,0:T(8,128)} %fusion.26.low_ref, f32[16,256]{1,0:T(8,128)} %right_ref.1, f32[1,256]{1,0:T(1,128)} %bitcast.7, ...), custom_call_target="tpu_custom_call" | custom-call | flops 16106127360 | bytes 2097152 | tf_op jit(solution)/shard_map/pallas_call | solution.py:98
  124.2 35.9 %all-gather.11.cloned.1.call-done = bf16[512,2048]{1,0:T(8,128)(2,1)} async-done(((bf16[512,256]{1,0:T(8,128)(2,1)}), bf16[512,2048]{1,0:T(8,128)(2,1)}) %all-gather.11.cloned.1.call-update) | async-done | bytes 2097168 | tf_op jit(solution)/shard_map/all_gather | solution.py:124
  160.1 4.4 convolution_convert_fusion.1
  165.5 28.5 %reduce-scatter.3.cloned.1.call-done = bf16[512,512]{1,0:T(8,128)(2,1)} async-done(((bf16[512,2048]{1,0:T(8,128)(2,1)}), bf16[512,512]{1,0:T(8,128)(2,1)}) %reduce-scatter.3.cloned.1.call-update) | async-done | bytes 524304 | tf_op jit(solution)/shard_map/reduce_scatter | solution.py:174
  194.0 1.2 fusion.10
  195.2 5.8 %psum.14 = f32[512]{0:T(512)S(1)} all-reduce(f32[512]{0:T(512)S(1)} %fusion.10), channel_id=1, replica_groups=mesh['grp'=2,'fs'=4,'tp'=4] {'tp'}, use_global_device_ids=true, to_apply=%region_3.0 | all-reduce | flops 512 | bytes 4096 | tf_op jit(solution)/shard_map/psum | solution.py:177
  201.0 2.1 fusion.13
  205.2 21.3 %all-gather.13.cloned.1.call-done = bf16[512,2048]{1,0:T(8,128)(2,1)} async-done(((bf16[512,512]{1,0:T(8,128)(2,1)}), bf16[512,2048]{1,0:T(8,128)(2,1)}) %all-gather.13.cloned.1.call-update) | async-done | bytes 2097168 | tf_op jit(solution)/shard_map/all_gather | solution.py:183
  226.5 2.2 fusion.3
  228.7 98.5 %all-gather.15.cloned.1.call-done = bf16[2048,1536]{1,0:T(8,128)(2,1)} async-done(((bf16[256,1536]{1,0:T(8,128)(2,1)}), bf16[2048,1536]{1,0:T(8,128)(2,1)}) %all-gather.15.cloned.1.call-update) | async-done | bytes 6291472 | tf_op jit(solution)/shard_map/all_gather | solution.py:124
  327.3 5.6 %fusion.6 = f32[512,1536]{1,0:T(8,128)S(1)} fusion(bf16[2048,1536]{1,0:T(8,128)(2,1)} %all-gather.15.cloned.1.call-done, bf16[512,2048]{1,0:T(8,128)(2,1)S(1)} %copy-done.4, f32[2048]{0:T(1024)S(1)} %copy-done.12, f32[512]{0:T(512)S(1)} %add_rsqrt_fusion.1), kind=kOutput, calls=%fused_computation.12 | convolution fusion | flops 3225419776 | bytes 11544576 | tf_op jit(solution)/shard_map/dot_general | solution.py:188
  332.9 1.4 fusion.33
  334.2 55.9 %all-gather.17.cloned.1.call-done = bf16[768,2048]{1,0:T(8,128)(2,1)} async-done(((bf16[768,256]{1,0:T(8,128)(2,1)}), bf16[768,2048]{1,0:T(8,128)(2,1)}) %all-gather.17.cloned.1.call-update) | async-done | bytes 3145744 | tf_op jit(solution)/shard_map/all_gather | solution.py:124
  390.1 7.5 %convolution_convert_fusion = bf16[512,2048]{1,0:T(8,128)(2,1)} fusion(bf16[768,2048]{1,0:T(8,128)(2,1)} %all-gather.17.cloned.1.call-done, f32[512,768]{1,0:T(8,128)} %get-tuple-element.12, f32[512,768]{1,0:T(8,128)S(1)} %get-tuple-element.11, f32[768]{0:T(1024)S(1)} %get-tuple-element.9, f32[768]{0:T(1024)S(1)} %get-tuple-element.10, ...), kind=kOutput, calls=%fused_computation.10 | convolution fusion | flops 1617952768 | bytes 8407040 | tf_op jit(solution)/shard_map/dot_general | solution.py:194
  398.5 28.7 %reduce-scatter.5.cloned.1.call-done = bf16[512,512]{1,0:T(8,128)(2,1)} async-done(((bf16[512,2048]{1,0:T(8,128)(2,1)}), bf16[512,512]{1,0:T(8,128)(2,1)}) %reduce-scatter.5.cloned.1.call-update) | async-done | bytes 524304 | tf_op jit(solution)/shard_map/reduce_scatter | solution.py:199
  427.2 1.2 fusion.14
  428.4 5.8 %psum.15 = f32[512]{0:T(512)S(1)} all-reduce(f32[512]{0:T(512)S(1)} %fusion.14), channel_id=1, replica_groups=mesh['grp'=2,'fs'=4,'tp'=4] {'tp'}, use_global_device_ids=true, to_apply=%region_7.8 | all-reduce | flops 512 | bytes 4096 | tf_op jit(solution)/shard_map/psum | solution.py:202
  434.2 2.1 fusion.17
  (56 shorter events, 7.1 us)
Async XLA Ops:
  6.5 197.7 %copy-start = (bf16[768,512]{1,0:T(8,128)(2,1)S(1)}, bf16[768,512]{1,0:T(8,128)(2,1)}, u32[]{:S(2)}) copy-start(bf16[768,512]{1,0:T(8,128)(2,1)} %param.37) | copy-start | bytes 2359300
  6.5 2.8 copy-start.7
  6.5 27.7 %all-gather.7.cloned.1.call-start = ((), (), s32[]{:S(2)}) async-start(), calls=%async_computation.2 | async-start | bytes 2621440 | tf_op jit(solution)/shard_map/all_gather | solution.py:151
  7.3 101.9 %all-gather.9.cloned.1.call-start = ((), (), s32[]{:S(2)}) async-start(), calls=%async_computation.3 | async-start | bytes 4718592 | tf_op jit(solution)/shard_map/all_gather | solution.py:124
  9.2 27.2 %copy-start.10 = (bf16[2048,16]{0,1:T(8,128)(2,1)S(1)}, bf16[2048,16]{0,1:T(8,128)(2,1)}, u32[]{:S(2)}) copy-start(bf16[2048,16]{0,1:T(8,128)(2,1)} %param.28) | copy-start | bytes 196612
  9.2 27.2 %copy-start.11 = (f32[2048]{0:T(1024)S(1)}, f32[2048]{0:T(1024)}, u32[]{:S(2)}) copy-start(f32[2048]{0:T(1024)} %param.20) | copy-start | bytes 24580
  9.3 150.8 %all-gather.11.cloned.1.call-start = ((), (), s32[]{:S(2)}) async-start(), calls=%async_computation.4 | async-start | bytes 2359296 | tf_op jit(solution)/shard_map/all_gather | solution.py:124
  10.1 183.9 %reduce-scatter.3.cloned.1.call-start = ((), (), s32[]{:S(2)}) async-start(), calls=%async_computation.5 | async-start | bytes 2621440 | tf_op jit(solution)/shard_map/reduce_scatter | solution.py:174
  34.2 2.3 copy-start.3
  164.5 36.5 %copy-start.2 = (bf16[512,512]{1,0:T(8,128)(2,1)S(1)}, bf16[512,512]{1,0:T(8,128)(2,1)}, u32[]{:S(2)}) copy-start(bf16[512,512]{1,0:T(8,128)(2,1)} %param.19) | copy-start | bytes 1572868
  164.5 38.7 %copy-start.5 = (bf16[512,768]{1,0:T(8,128)(2,1)S(1)}, bf16[512,768]{1,0:T(8,128)(2,1)}, u32[]{:S(2)}) copy-start(bf16[512,768]{1,0:T(8,128)(2,1)} %param.33) | copy-start | bytes 2359300
  164.5 38.7 %copy-start.6 = (bf16[512,768]{1,0:T(8,128)(2,1)S(1)}, bf16[512,768]{1,0:T(8,128)(2,1)}, u32[]{:S(2)}) copy-start(bf16[512,768]{1,0:T(8,128)(2,1)} %param.34) | copy-start | bytes 2359300
  164.5 62.0 %all-gather.13.cloned.1.call-start = ((), (), s32[]{:S(2)}) async-start(), calls=%async_computation.6 | async-start | bytes 2621440 | tf_op jit(solution)/shard_map/all_gather | solution.py:183
  203.1 2.0 copy-start.8
  203.1 2.0 copy-start.9
  203.1 124.1 %all-gather.15.cloned.1.call-start = ((), (), s32[]{:S(2)}) async-start(), calls=%async_computation.7 | async-start | bytes 7077888 | tf_op jit(solution)/shard_map/all_gather | solution.py:124
  204.2 123.1 %copy-start.12 = (f32[2048]{0:T(1024)S(1)}, f32[2048]{0:T(1024)}, u32[]{:S(2)}) copy-start(f32[2048]{0:T(1024)} %param.23) | copy-start | bytes 24580
  204.2 186.0 %all-gather.17.cloned.1.call-start = ((), (), s32[]{:S(2)}) async-start(), calls=%async_computation.8 | async-start | bytes 3538944 | tf_op jit(solution)/shard_map/all_gather | solution.py:124
  205.1 222.2 %reduce-scatter.5.cloned.1.call-start = ((), (), s32[]{:S(2)}) async-start(), calls=%async_computation.9 | async-start | bytes 2621440 | tf_op jit(solution)/shard_map/reduce_scatter | solution.py:199
  226.5 100.8 %copy-start.4 = (bf16[512,2048]{1,0:T(8,128)(2,1)S(1)}, bf16[512,2048]{1,0:T(8,128)(2,1)}, u32[]{:S(2)}) copy-start(bf16[512,2048]{1,0:T(8,128)(2,1)} %all-gather.13.cloned.1.call-done) | copy-start | bytes 6291460
  397.7 36.5 %copy-start.1 = (bf16[512,512]{1,0:T(8,128)(2,1)S(1)}, bf16[512,512]{1,0:T(8,128)(2,1)}, u32[]{:S(2)}) copy-start(bf16[512,512]{1,0:T(8,128)(2,1)} %fusion.13) | copy-start | bytes 1572868
Sparse Core Ops, SparseCore 0:
  8.9 25.2 all-gather.6
  36.3 72.7 all-gather.8
  111.2 48.8 all-gather.10
  164.6 29.3 reduce-scatter.2
  203.2 23.1 all-gather.12
  228.5 98.6 all-gather.14
  329.3 60.8 all-gather.16
  397.8 29.3 reduce-scatter.4

commit v2 on v1

--- a/solution.py
+++ b/solution.py
@@ -1,3 +1,5 @@
+import functools
+
 import jax
 import jax.numpy as jnp
 from jax import lax
@@ -117,11 +119,187 @@
     return summed
 
 
-def gather_parts(shard, dimension):
-    copies = lax.axis_size("grp")
-    part = shard.shape[dimension] // copies
-    own = lax.dynamic_slice_in_dim(shard, lax.axis_index("grp") * part, part, axis=dimension)
-    return lax.all_gather(own, ("fs", "grp"), axis=dimension, tiled=True)
+MESH = pl.DeviceIdType.MESH
+
+
+def piece(ref, dimension, owner, part, parts, full):
+    if dimension == 0:
+        height = ref.shape[0] // (parts * (lax.axis_size("fs") if full else 1))
+        first = (owner * parts + part) if full else part
+        return ref.at[pl.ds(pl.multiple_of(first * height, height), height), :]
+    height = ref.shape[0] // parts
+    rows = pl.ds(pl.multiple_of(part * height, height), height)
+    if not full:
+        return ref.at[rows, :]
+    width = ref.shape[1] // lax.axis_size("fs")
+    return ref.at[rows, pl.ds(pl.multiple_of(owner * width, width), width)]
+
+
+def gather_kernel(dimensions, *refs):
+    count = len(dimensions)
+    shards, maps = refs[:count], refs[count : 2 * count]
+    own_sem, line_send, line_recv, part_send, part_recv = refs[2 * count :]
+    line, parts = lax.axis_size("fs"), lax.axis_size("grp")
+    place, part = lax.axis_index("fs"), lax.axis_index("grp")
+
+    def there(way):
+        return place < line - 1 if way == 0 else place > 0
+
+    def toward(way):
+        return {"fs": place + 1 if way == 0 else place - 1}
+
+    def part_of(offset):
+        return lax.rem(part + offset, parts)
+
+    def line_copy(which, way, step):
+        owner = place - step if way == 0 else place + step
+        target = piece(maps[which], dimensions[which], owner, part, parts, True)
+        return pltpu.make_async_remote_copy(
+            src_ref=target,
+            dst_ref=target,
+            send_sem=line_send.at[which, way, step],
+            recv_sem=line_recv.at[which, way, step],
+            device_id=toward(way),
+            device_id_type=MESH,
+        )
+
+    def first_copy(which, way):
+        return pltpu.make_async_remote_copy(
+            src_ref=piece(shards[which], dimensions[which], place, part, parts, False),
+            dst_ref=piece(maps[which], dimensions[which], place, part, parts, True),
+            send_sem=line_send.at[which, way, 0],
+            recv_sem=line_recv.at[which, way, 0],
+            device_id=toward(way),
+            device_id_type=MESH,
+        )
+
+    def arrival(which, way, step):
+        owner = place - step - 1 if way == 0 else place + step + 1
+        target = piece(maps[which], dimensions[which], owner, part, parts, True)
+        return pltpu.make_async_remote_copy(
+            src_ref=target,
+            dst_ref=target,
+            send_sem=line_send.at[which, way, step],
+            recv_sem=line_recv.at[which, way, step],
+            device_id=toward(way),
+            device_id_type=MESH,
+        )
+
+    def part_copy(which, way, step, offset, coming):
+        owner = place - step - 1 if way == 0 else place + step + 1
+        mine = part_of(parts - offset) if coming else part
+        target = piece(maps[which], dimensions[which], owner, mine, parts, True)
+        return pltpu.make_async_remote_copy(
+            src_ref=target,
+            dst_ref=target,
+            send_sem=part_send.at[which, way, step, offset - 1],
+            recv_sem=part_recv.at[which, way, step, offset - 1],
+            device_id={"grp": part_of(offset)},
+            device_id_type=MESH,
+        )
+
+    def comes(way, step):
+        return place - step - 1 >= 0 if way == 0 else place + step + 1 < line
+
+    barrier = pltpu.get_barrier_semaphore()
+    for way in range(2):
+
+        @pl.when(there(way))
+        def _():
+            pl.semaphore_signal(barrier, inc=1, device_id=toward(way), device_id_type=MESH)
+
+    for offset in range(1, parts):
+        pl.semaphore_signal(
+            barrier, inc=1, device_id={"grp": part_of(offset)}, device_id_type=MESH
+        )
+    pl.semaphore_wait(
+        barrier, there(0).astype(jnp.int32) + there(1).astype(jnp.int32) + parts - 1
+    )
+
+    def begin(which):
+        for way in range(2):
+
+            @pl.when(there(way))
+            def _():
+                first_copy(which, way).start()
+
+    def own_copy(which):
+        height, width = shards[which].shape
+        if dimensions[which] == 0:
+            target = maps[which].at[pl.ds(pl.multiple_of(place * height, height), height), :]
+        else:
+            target = maps[which].at[:, pl.ds(pl.multiple_of(place * width, width), width)]
+        return pltpu.make_async_copy(shards[which], target, own_sem.at[which])
+
+    for which in range(min(2, count)):
+        begin(which)
+    for which in range(count):
+        own_copy(which).start()
+    for which in range(count):
+        if which + 2 < count:
+            begin(which + 2)
+
+        @pl.loop(0, line - 1)
+        def _(step):
+            for way in range(2):
+
+                @pl.when(comes(way, step))
+                def _():
+                    arrival(which, way, step).wait_recv()
+
+                    @pl.when(there(way))
+                    def _():
+                        line_copy(which, way, step + 1).start()
+
+                    for offset in range(1, parts):
+                        part_copy(which, way, step, offset, False).start()
+
+    for which in range(count):
+        own_copy(which).wait()
+        for way in range(2):
+
+            @pl.when(there(way))
+            def _():
+                first_copy(which, way).wait_send()
+
+        @pl.loop(0, line - 1)
+        def _(step):
+            for way in range(2):
+
+                @pl.when(comes(way, step))
+                def _():
+                    @pl.when(there(way))
+                    def _():
+                        line_copy(which, way, step + 1).wait_send()
+
+                    for offset in range(1, parts):
+                        part_copy(which, way, step, offset, False).wait_send()
+                        part_copy(which, way, step, offset, True).wait_recv()
+
+
+def gather_maps(shards, dimensions, identity):
+    line, parts = lax.axis_size("fs"), lax.axis_size("grp")
+    count = len(shards)
+    shapes = [
+        (shard.shape[0] * line, shard.shape[1]) if dimension == 0 else (shard.shape[0], shard.shape[1] * line)
+        for shard, dimension in zip(shards, dimensions)
+    ]
+    sent = sum(2 * shard.size for shard in shards) * (line - 1)
+    return pl.pallas_call(
+        functools.partial(gather_kernel, dimensions),
+        out_shape=[jax.ShapeDtypeStruct(shape, jnp.bfloat16) for shape in shapes],
+        in_specs=[pl.BlockSpec(memory_space=pltpu.VMEM)] * count,
+        out_specs=[pl.BlockSpec(memory_space=pl.ANY)] * count,
+        scratch_shapes=[
+            pltpu.SemaphoreType.DMA((count,)),
+            pltpu.SemaphoreType.DMA((count, 2, line)),
+            pltpu.SemaphoreType.DMA((count, 2, line)),
+            pltpu.SemaphoreType.DMA((count, 2, line, max(parts - 1, 1))),
+            pltpu.SemaphoreType.DMA((count, 2, line, max(parts - 1, 1))),
+        ],
+        compiler_params=pltpu.CompilerParams(collective_id=identity, has_side_effects=True),
+        cost_estimate=pl.CostEstimate(flops=0, bytes_accessed=30 * sent, transcendentals=0),
+    )(*shards)
 
 
 def on_device(
@@ -150,16 +328,18 @@
     full_width = own_columns * lax.axis_size("tp")
     full_rows = lax.all_gather(block_source_tensor, "tp", axis=1, tiled=True)
     normed = norm_rows(full_rows.astype(jnp.float32), attend_initial_norm_gain).astype(jnp.bfloat16)
-    qkv_map = gather_parts(
-        jnp.concatenate([question_map, address_map, payload_weights_map], axis=1), 0
-    )
-    qk_columns = question_map.shape[1]
-    projected = jnp.dot(normed, qkv_map, preferred_element_type=jnp.float32).astype(jnp.bfloat16)
+    question_full, address_full, payload_full, combining_full = gather_maps(
+        (question_map, address_map, payload_weights_map, combining_map), (0, 0, 0, 1), 1
+    )
+    query, key, value = (
+        jnp.dot(normed, full, preferred_element_type=jnp.float32).astype(jnp.bfloat16)
+        for full in (question_full, address_full, payload_full)
+    )
     low_rank = jnp.dot(normed, fading_left_factor, preferred_element_type=jnp.float32)
     head_out = mixing(
-        projected[:, :qk_columns],
-        projected[:, qk_columns : 2 * qk_columns],
-        projected[:, 2 * qk_columns :],
+        query,
+        key,
+        value,
         low_rank,
         fading_right_factor,
         fading_valve_constant[None],
@@ -168,32 +348,39 @@
     )
     partials = jnp.dot(
         head_out,
-        gather_parts(combining_map, 1),
+        combining_full,
         preferred_element_type=jnp.float32,
     )
+    partials = partials.astype(jnp.bfloat16)
+    valve_shard, partials = lax.optimization_barrier((valve_map, partials))
+    (valve_full,) = gather_maps((valve_shard,), (0,), 2)
     mixed = lax.psum_scatter(
-        partials.astype(jnp.bfloat16), "tp", scatter_dimension=1, tiled=True
-    ).astype(jnp.float32)
+        partials, "tp", scatter_dimension=1, tiled=True
+    )
+    mixed, valve_full = lax.optimization_barrier((mixed, valve_full))
+    mixed = mixed.astype(jnp.float32)
     squares = lax.psum(jnp.sum(mixed * mixed, axis=1), "tp")
     own_gain = lax.dynamic_slice_in_dim(attend_final_norm_gain, tp_index * own_columns, own_columns)
     first = (
         block_source_tensor.astype(jnp.float32)
         + mixed * lax.rsqrt(squares / full_width + epsilon)[:, None] * own_gain
     ).astype(jnp.bfloat16)
+    widening_shard, narrowing_shard, first = lax.optimization_barrier(
+        (widening_map, narrowing_map, first)
+    )
+    widening_full, narrowing_full = gather_maps((widening_shard, narrowing_shard), (0, 1), 3)
     first_rows = lax.all_gather(first, "tp", axis=1, tiled=True)
     ffn_in = norm_rows(first_rows.astype(jnp.float32), dense_initial_norm_gain).astype(jnp.bfloat16)
 
-    gate_up_map = gather_parts(jnp.concatenate([valve_map, widening_map], axis=1), 0)
-    units = valve_map.shape[1]
-    gate_up = jnp.dot(ffn_in, gate_up_map, preferred_element_type=jnp.float32)
-    gate_pre, up_pre = gate_up[:, :units], gate_up[:, units:]
+    gate_pre = jnp.dot(ffn_in, valve_full, preferred_element_type=jnp.float32)
+    up_pre = jnp.dot(ffn_in, widening_full, preferred_element_type=jnp.float32)
     hidden = (
         jax.nn.silu(causal_taps(gate_pre, valve_conv_stencil))
         * causal_taps(up_pre, widening_conv_stencil)
     ).astype(jnp.bfloat16)
     down_partials = jnp.dot(
         hidden,
-        gather_parts(narrowing_map, 1),
+        narrowing_full,
         preferred_element_type=jnp.float32,
     )
     channel = lax.psum_scatter(

time: 444 us -> 285 us (0.64)
  waiting for transfers between devices: 365 us -> 29.7 us
  Pallas kernels: 8.75 us -> 195 us
  local copies, waits for them, and re-layouts: 6.37 us -> 1.71 us
    all_gather x4 -> x0, waiting for transfers between devices: 262 us -> none  [gather_parts(): return lax.all_gather(own, ('fs', 'grp'), axis=dimension, tiled=True)]
    pallas_call x0 -> x3, Pallas kernels: none -> 186 us  [gather_maps(): pl.pallas_call(functools.partial(gather_kernel, dimensions), out_shape=[j...]
    reduce_scatter x1, waiting for transfers between devices: 28.5 us -> 0.02 us  [on_device(): mixed = lax.psum_scatter(partials, 'tp', scatter_dimension=1, tiled=True)]
    all_gather x1, waiting for transfers between devices: 24.1 us -> 0.02 us  [on_device(): full_rows = lax.all_gather(block_source_tensor, 'tp', axis=1, tiled=True)]
    all_gather x1, waiting for transfers between devices: 21.3 us -> 0.02 us  [on_device(): first_rows = lax.all_gather(first, 'tp', axis=1, tiled=True)]
    dot_general x4 -> x7, matrix products: 22.1 us -> 20 us  [the longest x3 6.77 us: on_device(): jnp.dot(normed, full, preferred_element_type=jnp.float32)]
  transfers between devices with their start and end apart: 8 -> 4, of which waited for: 8 -> 1; matrix products, arithmetic and copies ran while one was open for 6% -> 1% of each run, Pallas kernels for 2% -> 66%
where the time goes in v2:
time: 285 us; the launch traced here: 284 us
  Pallas kernels  195 us (68%)
  waiting for transfers between devices  29.7 us (10%)
  matrix products  21.5 us (8%)
  between operations  13.3 us (5%)
  blocking collectives  11.4 us (4%)
  other arithmetic  11 us (4%)
    pallas_call x3, Pallas kernels, gather_maps(): pl.pallas_call(functools.partial(gather_kernel, dimensions), out_shape=[j...  186 us
    reduce_scatter x1, waiting for transfers between devices, on_device(): lax.psum_scatter(down_partials.astype(jnp.bfloat16), 'tp', scatter_dimens...  28.9 us
    pallas_call x1, Pallas kernels, mixing(): pl.pallas_call(mixing_kernel, out_shape=jax.ShapeDtypeStruct(value.shape,...  8.86 us
    dot_general x3, matrix products, on_device(): jnp.dot(normed, full, preferred_element_type=jnp.float32)  6.77 us
    psum x1, blocking collectives, on_device(): channel_squares = lax.psum(jnp.sum(channel * channel, axis=1), 'tp')  5.76 us
  transfers between devices with their start and end apart: 4, of which 1 were waited for; matrix products, arithmetic and copies ran while one was open for 1% of the time, Pallas kernels for 66%

profile of v2, /device:TPU:0, one launch (start us, length us, event | category | flops | bytes accessed | tf_op | source)
XLA Modules:
  0.0 284.1 jit_solution(6021501643330836944)
XLA Ops:
  6.5 0.7 all-gather.3.cloned.1.call-update
  7.3 76.5 %shard_map.181 = (bf16[2048,256]{1,0:T(8,128)(2,1)}, bf16[2048,256]{1,0:T(8,128)(2,1)}, bf16[2048,512]{1,0:T(8,128)(2,1)}, bf16[512,2048]{1,0:T(8,128)(2,1)}) custom-call(bf16[512,256]{1,0:T(8,128)(2,1)} %refs_0_.1, bf16[512,256]{1,0:T(8,128)(2,1)} %refs_1_.1, bf16[512,512]{1,0:T(8,128)(2,1)} %refs_2_.1, bf16[512,512]{1,0:T(8,128)(2,1)} %refs_3_.1), custom_call_target="tpu_custom_call" | custom-call | bytes 141557760 | tf_op jit(solution)/shard_map/pallas_call | solution.py:288
  83.9 2.2 fusion
  86.1 3.8 %convolution_convert_fusion.2.v_ref = bf16[512,512]{1,0:T(8,128)(2,1)} fusion(bf16[2048,512]{1,0:T(8,128)(2,1)} %get-tuple-element.20, bf16[512,2048]{1,0:T(8,128)(2,1)S(1)} %copy-done.5, f32[2048]{0:T(1024)S(1)} %copy-done.13, f32[512]{0:T(512)S(1)} %add_rsqrt_fusion.3), kind=kOutput, calls=%fused_computation.17 | convolution fusion | flops 1078198272 | bytes 4728832 | tf_op jit(solution)/shard_map/dot_general | solution.py:335
  89.9 1.5 convolution_convert_fusion.3.k_ref
  91.4 1.5 convolution_convert_fusion.4.q_ref
  92.9 1.5 fusion.27.low_ref
  94.4 8.9 %shard_map.182 = bf16[512,512]{1,0:T(8,128)(2,1)} custom-call(bf16[512,256]{1,0:T(8,128)(2,1)} %convolution_convert_fusion.4.q_ref, bf16[512,256]{1,0:T(8,128)(2,1)} %convolution_convert_fusion.3.k_ref, bf16[512,512]{1,0:T(8,128)(2,1)} %convolution_convert_fusion.2.v_ref, f32[512,16]{1,0:T(8,128)} %fusion.27.low_ref, f32[16,256]{1,0:T(8,128)} %right_ref.1, ...), custom_call_target="tpu_custom_call" | custom-call | flops 16106127360 | bytes 2097152 | tf_op jit(solution)/shard_map/pallas_call | solution.py:100
  103.3 3.7 %convolution_convert_fusion.1 = bf16[512,2048]{1,0:T(8,128)(2,1)} fusion(bf16[512,512]{1,0:T(8,128)(2,1)} %shard_map.182, bf16[512,2048]{1,0:T(8,128)(2,1)S(1)} %copy-done.10), kind=kOutput, calls=%fused_computation.11 | convolution fusion | flops 1074790400 | bytes 4718592 | tf_op jit(solution)/shard_map/dot_general | solution.py:349
  107.0 0.8 dynamic_slice.6
  107.8 35.8 %shard_map.183 = bf16[2048,768]{1,0:T(8,128)(2,1)} custom-call(bf16[512,768]{1,0:T(8,128)(2,1)} %refs_0_.2), custom_call_target="tpu_custom_call" | custom-call | bytes 70778880 | tf_op jit(solution)/shard_map/pallas_call | solution.py:288
  143.7 1.2 fusion.6
  144.9 5.7 %psum.14 = f32[512]{0:T(512)S(1)} all-reduce(f32[512]{0:T(512)S(1)} %fusion.6), channel_id=1, replica_groups=mesh['grp'=2,'fs'=4,'tp'=4] {'tp'}, use_global_device_ids=true, to_apply=%region_3.0 | all-reduce | flops 512 | bytes 4096 | tf_op jit(solution)/shard_map/psum | solution.py:362
  150.6 2.1 fusion.9
  152.9 74.1 %shard_map.184 = (bf16[2048,768]{1,0:T(8,128)(2,1)}, bf16[768,2048]{1,0:T(8,128)(2,1)}) custom-call(bf16[512,768]{1,0:T(8,128)(2,1)} %refs_0_.3, bf16[768,512]{1,0:T(8,128)(2,1)} %refs_1_.2), custom_call_target="tpu_custom_call" | custom-call | bytes 141557760 | tf_op jit(solution)/shard_map/pallas_call | solution.py:288
  227.0 2.1 fusion.3
  229.2 3.6 %fusion.23 = f32[512,768]{1,0:T(8,128)S(1)} fusion(bf16[2048,768]{1,0:T(8,128)(2,1)S(1)} %copy-done.2, bf16[512,2048]{1,0:T(8,128)(2,1)} %all-gather.5.cloned.1.call-done, f32[2048]{0:T(1024)S(1)} %copy-done.14, f32[512]{0:T(512)S(1)} %add_rsqrt_fusion.1), kind=kOutput, calls=%fused_computation.36 | convolution fusion | flops 1614807040 | bytes 6825984 | tf_op jit(solution)/shard_map/dot_general | solution.py:375
  232.8 1.9 fusion.21
  234.7 4.1 %convolution_convert_fusion = bf16[512,2048]{1,0:T(8,128)(2,1)} fusion(bf16[768,2048]{1,0:T(8,128)(2,1)S(1)} %copy-done.8, f32[512,768]{1,0:T(8,128)S(1)} %fusion.21, f32[512,768]{1,0:T(8,128)S(1)} %fusion.23, f32[768]{0:T(1024)S(1)} %get-tuple-element.35, f32[768]{0:T(1024)S(1)} %get-tuple-element.36, f32[768]{0:T(1024)S(1)} %get-tuple-element.34, ...), kind=kOutput, calls=%fused_computation.10 | convolution fusion | flops 1617952768 | bytes 8407040 | tf_op jit(solution)/shard_map/dot_general | solution.py:381
  238.8 0.8 dynamic_slice.7
  239.6 28.9 %reduce-scatter.5.cloned.1.call-done = bf16[512,512]{1,0:T(8,128)(2,1)} async-done(((bf16[512,2048]{1,0:T(8,128)(2,1)}), bf16[512,512]{1,0:T(8,128)(2,1)}) %reduce-scatter.5.cloned.1.call-update) | async-done | bytes 524304 | tf_op jit(solution)/shard_map/reduce_scatter | solution.py:386
  268.5 1.2 fusion.10
  269.7 5.8 %psum.15 = f32[512]{0:T(512)S(1)} all-reduce(f32[512]{0:T(512)S(1)} %fusion.10), channel_id=1, replica_groups=mesh['grp'=2,'fs'=4,'tp'=4] {'tp'}, use_global_device_ids=true, to_apply=%region_7.8 | all-reduce | flops 512 | bytes 4096 | tf_op jit(solution)/shard_map/psum | solution.py:389
  275.5 2.1 fusion.13
  (47 shorter events, 0.4 us)
Async XLA Ops:
  6.5 86.4 %copy-start = (bf16[2048,16]{0,1:T(8,128)(2,1)S(1)}, bf16[2048,16]{0,1:T(8,128)(2,1)}, u32[]{:S(2)}) copy-start(bf16[2048,16]{0,1:T(8,128)(2,1)} %param.28) | copy-start | bytes 196612
  6.5 79.6 %copy-start.13 = (f32[2048]{0:T(1024)S(1)}, f32[2048]{0:T(1024)}, u32[]{:S(2)}) copy-start(f32[2048]{0:T(1024)} %param.20) | copy-start | bytes 24580
  6.5 77.3 %all-gather.3.cloned.1.call-start = ((), (), s32[]{:S(2)}) async-start(), calls=%async_computation.2 | async-start | bytes 2621440 | tf_op jit(solution)/shard_map/all_gather | solution.py:329
  7.3 136.4 %reduce-scatter.3.cloned.1.call-start = ((), (), s32[]{:S(2)}) async-start(), calls=%async_computation.3 | async-start | bytes 2621440 | tf_op jit(solution)/shard_map/reduce_scatter | solution.py:357
  83.9 2.3 copy-start.5
  86.1 3.8 %copy-start.12 = (bf16[2048,256]{1,0:T(8,128)(2,1)S(1)}, bf16[2048,256]{1,0:T(8,128)(2,1)}, u32[]{:S(2)}) copy-start(bf16[2048,256]{1,0:T(8,128)(2,1)} %get-tuple-element.19) | copy-start | bytes 3145732
  89.9 1.5 copy-start.11
  94.4 8.9 %copy-start.10 = (bf16[512,2048]{1,0:T(8,128)(2,1)S(1)}, bf16[512,2048]{1,0:T(8,128)(2,1)}, u32[]{:S(2)}) copy-start(bf16[512,2048]{1,0:T(8,128)(2,1)} %get-tuple-element.21) | copy-start | bytes 6291460
  107.0 120.1 %all-gather.5.cloned.1.call-start = ((), (), s32[]{:S(2)}) async-start(), calls=%async_computation.4 | async-start | bytes 2621440 | tf_op jit(solution)/shard_map/all_gather | solution.py:372
  107.8 42.8 %copy-start.3 = (bf16[512,512]{1,0:T(8,128)(2,1)S(1)}, bf16[512,512]{1,0:T(8,128)(2,1)}, u32[]{:S(2)}) copy-start(bf16[512,512]{1,0:T(8,128)(2,1)} %param.19) | copy-start | bytes 1572868
  143.6 9.1 %copy-start.6 = (bf16[3,768]{1,0:T(4,128)(2,1)S(1)}, bf16[3,768]{1,0:T(4,128)(2,1)}, u32[]{:S(2)}) copy-start(bf16[3,768]{1,0:T(4,128)(2,1)} %param.35) | copy-start | bytes 13828
  143.6 9.1 %copy-start.7 = (bf16[3,768]{1,0:T(4,128)(2,1)S(1)}, bf16[3,768]{1,0:T(4,128)(2,1)}, u32[]{:S(2)}) copy-start(bf16[3,768]{1,0:T(4,128)(2,1)} %param.36) | copy-start | bytes 13828
  152.7 76.4 %copy-start.2 = (bf16[2048,768]{1,0:T(8,128)(2,1)S(1)}, bf16[2048,768]{1,0:T(8,128)(2,1)}, u32[]{:S(2)}) copy-start(bf16[2048,768]{1,0:T(8,128)(2,1)} %shard_map.183) | copy-start | bytes 9437188
  152.7 76.5 %copy-start.14 = (f32[2048]{0:T(1024)S(1)}, f32[2048]{0:T(1024)}, u32[]{:S(2)}) copy-start(f32[2048]{0:T(1024)} %param.23) | copy-start | bytes 24580
  152.7 115.8 %reduce-scatter.5.cloned.1.call-start = ((), (), s32[]{:S(2)}) async-start(), calls=%async_computation.5 | async-start | bytes 2621440 | tf_op jit(solution)/shard_map/reduce_scatter | solution.py:386
  229.1 3.6 %copy-start.4 = (bf16[512,2048]{1,0:T(8,128)(2,1)S(1)}, bf16[512,2048]{1,0:T(8,128)(2,1)}, u32[]{:S(2)}) copy-start(bf16[512,2048]{1,0:T(8,128)(2,1)} %all-gather.5.cloned.1.call-done) | copy-start | bytes 6291460
  229.1 3.6 %copy-start.9 = (bf16[2048,768]{1,0:T(8,128)(2,1)S(1)}, bf16[2048,768]{1,0:T(8,128)(2,1)}, u32[]{:S(2)}) copy-start(bf16[2048,768]{1,0:T(8,128)(2,1)} %get-tuple-element.29) | copy-start | bytes 9437188
  232.8 1.9 copy-start.8
  238.7 36.8 %copy-start.1 = (bf16[512,512]{1,0:T(8,128)(2,1)S(1)}, bf16[512,512]{1,0:T(8,128)(2,1)}, u32[]{:S(2)}) copy-start(bf16[512,512]{1,0:T(8,128)(2,1)} %fusion.9) | copy-start | bytes 1572868
Sparse Core Ops, SparseCore 0:
  8.9 25.2 all-gather.2
  107.1 29.1 reduce-scatter.2
  152.8 21.3 all-gather.4
  238.9 29.5 reduce-scatter.4

commit v3 on v2

--- a/solution.py
+++ b/solution.py
@@ -122,23 +122,147 @@
 MESH = pl.DeviceIdType.MESH
 
 
-def piece(ref, dimension, owner, part, parts, full):
-    if dimension == 0:
-        height = ref.shape[0] // (parts * (lax.axis_size("fs") if full else 1))
-        first = (owner * parts + part) if full else part
-        return ref.at[pl.ds(pl.multiple_of(first * height, height), height), :]
-    height = ref.shape[0] // parts
-    rows = pl.ds(pl.multiple_of(part * height, height), height)
-    if not full:
+def piece(ref, dimension, owner, part, full, cut, cuts):
+    parts, line = lax.axis_size("grp"), lax.axis_size("fs")
+    height = ref.shape[0] // (parts * cuts * (line if full and dimension == 0 else 1))
+    first = part * cuts + cut
+    if full and dimension == 0:
+        first = owner * parts * cuts + first
+    rows = pl.ds(pl.multiple_of(first * height, height), height)
+    if not full or dimension == 0:
         return ref.at[rows, :]
-    width = ref.shape[1] // lax.axis_size("fs")
+    width = ref.shape[1] // line
     return ref.at[rows, pl.ds(pl.multiple_of(owner * width, width), width)]
 
 
-def gather_kernel(dimensions, *refs):
+def cuts_of(shard):
+    parts = lax.axis_size("grp")
+    cuts = 1
+    while shard.size // (parts * 2 * cuts) >= 48 * 1024 and shard.shape[0] % (parts * 2 * cuts * 16) == 0:
+        cuts *= 2
+    return cuts
+
+
+def gather_kernel(dimensions, cuts, spread, summed, *refs):
     count = len(dimensions)
-    shards, maps = refs[:count], refs[count : 2 * count]
-    own_sem, line_send, line_recv, part_send, part_recv = refs[2 * count :]
+    refs = list(refs)
+
+    def take(number):
+        taken = refs[:number]
+        del refs[:number]
+        return taken
+
+    shards, block, partial = take(count), take(spread), take(summed)
+    maps, rows_out = take(count), take(spread)
+    total_out, squares_out = take(2) if summed else (None, None)
+    if count:
+        own_sem, line_send, line_recv, part_send, part_recv = take(5)
+    if spread:
+        spread_own, spread_send, spread_recv = take(3)
+    if summed:
+        pair_in, chip_sum, chip_in, squares_own, squares_in = take(5)
+        pair_send, pair_recv, chip_send, chip_recv, squares_send, squares_recv = take(6)
+    ranks, rank = lax.axis_size("tp"), lax.axis_index("tp")
+    chips, chip, core = ranks // 2, rank // 2, lax.rem(rank, 2)
+
+    def rank_at(offset):
+        return lax.rem(rank + offset, ranks)
+
+    def columns_of(ref, owner):
+        width = ref.shape[1] // ranks
+        return ref.at[:, pl.ds(pl.multiple_of(owner * width, width), width)]
+
+    def spread_copy(offset, owner):
+        return pltpu.make_async_remote_copy(
+            src_ref=block[0],
+            dst_ref=columns_of(rows_out[0], owner),
+            send_sem=spread_send.at[offset],
+            recv_sem=spread_recv.at[offset],
+            device_id={"tp": rank_at(offset)},
+            device_id_type=MESH,
+        )
+
+    def spread_local():
+        return pltpu.make_async_copy(block[0], columns_of(rows_out[0], rank), spread_own)
+
+    def pair_copy(target):
+        return pltpu.make_async_remote_copy(
+            src_ref=columns_of(partial[0], target * 2 + 1 - core),
+            dst_ref=pair_in.at[target],
+            send_sem=pair_send.at[target],
+            recv_sem=pair_recv.at[target],
+            device_id={"tp": chip * 2 + 1 - core},
+            device_id_type=MESH,
+        )
+
+    def chip_copy(offset):
+        return pltpu.make_async_remote_copy(
+            src_ref=chip_sum.at[offset],
+            dst_ref=chip_in.at[offset],
+            send_sem=chip_send.at[offset],
+            recv_sem=chip_recv.at[offset],
+            device_id={"tp": lax.rem(chip + offset, chips) * 2 + core},
+            device_id_type=MESH,
+        )
+
+    def squares_copy(offset):
+        return pltpu.make_async_remote_copy(
+            src_ref=squares_own,
+            dst_ref=squares_in.at[offset],
+            send_sem=squares_send.at[offset],
+            recv_sem=squares_recv.at[offset],
+            device_id={"tp": rank_at(offset)},
+            device_id_type=MESH,
+        )
+
+    def sum_pairs():
+        for target in range(chips):
+            pair_copy(target).wait_recv()
+        for offset in list(range(1, chips)) + [0]:
+            target = lax.rem(chip + offset, chips)
+            both = (
+                columns_of(partial[0], target * 2 + core)[...].astype(jnp.float32)
+                + pair_in[target].astype(jnp.float32)
+            )
+            if offset:
+                chip_sum[offset] = both.astype(jnp.bfloat16)
+                chip_copy(offset).start()
+            else:
+                total_out[...] = both
+
+    def sum_chips():
+        for offset in range(1, chips):
+            chip_copy(offset).wait_recv()
+            total_out[...] += chip_in[offset].astype(jnp.float32)
+        total = total_out[...]
+        squares_own[...] = lax.dot_general(
+            jnp.ones((8, total.shape[1]), jnp.float32),
+            total * total,
+            (((1,), (1,)), ((), ())),
+            precision=careful_evaluation,
+            preferred_element_type=jnp.float32,
+        )
+        for offset in range(1, ranks):
+            squares_copy(offset).start()
+        summed_squares = squares_own[...]
+        for offset in range(1, ranks):
+            squares_copy(offset).wait_recv()
+            summed_squares = summed_squares + squares_in[offset]
+        squares_out[...] = lax.dot_general(
+            summed_squares,
+            jnp.full((8, 128), 0.125, jnp.float32),
+            (((0,), (0,)), ((), ())),
+            precision=careful_evaluation,
+            preferred_element_type=jnp.float32,
+        )
+        for target in range(chips):
+            pair_copy(target).wait_send()
+        for offset in range(1, chips):
+            chip_copy(offset).wait_send()
+        for offset in range(1, ranks):
+            squares_copy(offset).wait_send()
+
+    pieces = [(which, cut) for which in range(count) for cut in range(cuts[which])]
     line, parts = lax.axis_size("fs"), lax.axis_size("grp")
     place, part = lax.axis_index("fs"), lax.axis_index("grp")
 
@@ -151,49 +275,53 @@
     def part_of(offset):
         return lax.rem(part + offset, parts)
 
-    def line_copy(which, way, step):
+    def at(refs, unit, owner, half, full):
+        which, cut = pieces[unit]
+        return piece(refs[which], dimensions[which], owner, half, full, cut, cuts[which])
+
+    def line_copy(unit, way, step):
         owner = place - step if way == 0 else place + step
-        target = piece(maps[which], dimensions[which], owner, part, parts, True)
+        target = at(maps, unit, owner, part, True)
         return pltpu.make_async_remote_copy(
             src_ref=target,
             dst_ref=target,
-            send_sem=line_send.at[which, way, step],
-            recv_sem=line_recv.at[which, way, step],
+            send_sem=line_send.at[unit, way, step],
+            recv_sem=line_recv.at[unit, way, step],
             device_id=toward(way),
             device_id_type=MESH,
         )
 
-    def first_copy(which, way):
-        return pltpu.make_async_remote_copy(
-            src_ref=piece(shards[which], dimensions[which], place, part, parts, False),
-            dst_ref=piece(maps[which], dimensions[which], place, part, parts, True),
-            send_sem=line_send.at[which, way, 0],
-            recv_sem=line_recv.at[which, way, 0],
+    def first_copy(unit, way):
+        return pltpu.make_async_remote_copy(
+            src_ref=at(shards, unit, place, part, False),
+            dst_ref=at(maps, unit, place, part, True),
+            send_sem=line_send.at[unit, way, 0],
+            recv_sem=line_recv.at[unit, way, 0],
             device_id=toward(way),
             device_id_type=MESH,
         )
 
-    def arrival(which, way, step):
+    def arrival(unit, way, step):
         owner = place - step - 1 if way == 0 else place + step + 1
-        target = piece(maps[which], dimensions[which], owner, part, parts, True)
+        target = at(maps, unit, owner, part, True)
         return pltpu.make_async_remote_copy(
             src_ref=target,
             dst_ref=target,
-            send_sem=line_send.at[which, way, step],
-            recv_sem=line_recv.at[which, way, step],
+            send_sem=line_send.at[unit, way, step],
+            recv_sem=line_recv.at[unit, way, step],
             device_id=toward(way),
             device_id_type=MESH,
         )
 
-    def part_copy(which, way, step, offset, coming):
+    def part_copy(unit, way, step, offset, coming):
         owner = place - step - 1 if way == 0 else place + step + 1
         mine = part_of(parts - offset) if coming else part
-        target = piece(maps[which], dimensions[which], owner, mine, parts, True)
+        target = at(maps, unit, owner, mine, True)
         return pltpu.make_async_remote_copy(
             src_ref=target,
             dst_ref=target,
-            send_sem=part_send.at[which, way, step, offset - 1],
-            recv_sem=part_recv.at[which, way, step, offset - 1],
+            send_sem=part_send.at[unit, way, step, offset - 1],
+            recv_sem=part_recv.at[unit, way, step, offset - 1],
             device_id={"grp": part_of(offset)},
             device_id_type=MESH,
         )
@@ -202,26 +330,36 @@
         return place - step - 1 >= 0 if way == 0 else place + step + 1 < line
 
     barrier = pltpu.get_barrier_semaphore()
-    for way in range(2):
-
-        @pl.when(there(way))
-        def _():
-            pl.semaphore_signal(barrier, inc=1, device_id=toward(way), device_id_type=MESH)
-
-    for offset in range(1, parts):
-        pl.semaphore_signal(
-            barrier, inc=1, device_id={"grp": part_of(offset)}, device_id_type=MESH
-        )
-    pl.semaphore_wait(
-        barrier, there(0).astype(jnp.int32) + there(1).astype(jnp.int32) + parts - 1
-    )
-
-    def begin(which):
+    expected = 0
+    if count:
         for way in range(2):
 
             @pl.when(there(way))
             def _():
-                first_copy(which, way).start()
+                pl.semaphore_signal(barrier, inc=1, device_id=toward(way), device_id_type=MESH)
+
+        for offset in range(1, parts):
+            pl.semaphore_signal(
+                barrier, inc=1, device_id={"grp": part_of(offset)}, device_id_type=MESH
+            )
+        expected = there(0).astype(jnp.int32) + there(1).astype(jnp.int32) + parts - 1
+    if spread or summed:
+        for offset in range(1, ranks):
+            pl.semaphore_signal(
+                barrier, inc=1, device_id={"tp": rank_at(offset)}, device_id_type=MESH
+            )
+        expected = expected + ranks - 1
+    pl.semaphore_wait(barrier, expected)
+    if summed:
+        for target in range(chips):
+            pair_copy(target).start()
+
+    def begin(unit):
+        for way in range(2):
+
+            @pl.when(there(way))
+            def _():
+                first_copy(unit, way).start()
 
     def own_copy(which):
         height, width = shards[which].shape
@@ -231,36 +369,52 @@
             target = maps[which].at[:, pl.ds(pl.multiple_of(place * width, width), width)]
         return pltpu.make_async_copy(shards[which], target, own_sem.at[which])
 
-    for which in range(min(2, count)):
-        begin(which)
+    def pass_on(unit, step):
+        for way in range(2):
+
+            @pl.when(comes(way, step))
+            def _():
+                arrival(unit, way, step).wait_recv()
+
+                @pl.when(there(way))
+                def _():
+                    line_copy(unit, way, step + 1).start()
+
+                for offset in range(1, parts):
+                    part_copy(unit, way, step, offset, False).start()
+
+    if count:
+        begin(0)
+    if spread:
+        for offset in range(1, ranks):
+            spread_copy(offset, rank).start()
+        spread_local().start()
     for which in range(count):
         own_copy(which).start()
-    for which in range(count):
-        if which + 2 < count:
-            begin(which + 2)
-
-        @pl.loop(0, line - 1)
-        def _(step):
-            for way in range(2):
-
-                @pl.when(comes(way, step))
-                def _():
-                    arrival(which, way, step).wait_recv()
-
-                    @pl.when(there(way))
-                    def _():
-                        line_copy(which, way, step + 1).start()
-
-                    for offset in range(1, parts):
-                        part_copy(which, way, step, offset, False).start()
-
+    if summed:
+        sum_pairs()
+    for tick in range(len(pieces) + line - 2 if count else 0):
+        if tick + 1 < len(pieces):
+            begin(tick + 1)
+        for step in range(line - 1):
+            if 0 <= tick - step < len(pieces):
+                pass_on(tick - step, step)
+
+    if summed:
+        sum_chips()
+    if spread:
+        spread_local().wait()
+        for offset in range(1, ranks):
+            spread_copy(offset, rank).wait_send()
+            spread_copy(offset, rank_at(ranks - offset)).wait_recv()
     for which in range(count):
         own_copy(which).wait()
+    for unit in range(len(pieces)):
         for way in range(2):
 
             @pl.when(there(way))
             def _():
-                first_copy(which, way).wait_send()
+                first_copy(unit, way).wait_send()
 
         @pl.loop(0, line - 1)
         def _(step):
@@ -270,36 +424,60 @@
                 def _():
                     @pl.when(there(way))
                     def _():
-                        line_copy(which, way, step + 1).wait_send()
+                        line_copy(unit, way, step + 1).wait_send()
 
                     for offset in range(1, parts):
-                        part_copy(which, way, step, offset, False).wait_send()
-                        part_copy(which, way, step, offset, True).wait_recv()
-
-
-def gather_maps(shards, dimensions, identity):
-    line, parts = lax.axis_size("fs"), lax.axis_size("grp")
+                        part_copy(unit, way, step, offset, False).wait_send()
+                        part_copy(unit, way, step, offset, True).wait_recv()
+
+
+def exchange(shards, dimensions, identity, block=None, partial=None):
+    line, parts, ranks = lax.axis_size("fs"), lax.axis_size("grp"), lax.axis_size("tp")
     count = len(shards)
+    cuts = [cuts_of(shard) for shard in shards]
+    units = sum(cuts)
+    spread, summed = int(block is not None), int(partial is not None)
+    vmem, anywhere = pl.BlockSpec(memory_space=pltpu.VMEM), pl.BlockSpec(memory_space=pl.ANY)
+    operands = list(shards)
     shapes = [
-        (shard.shape[0] * line, shard.shape[1]) if dimension == 0 else (shard.shape[0], shard.shape[1] * line)
+        jax.ShapeDtypeStruct(
+            (shard.shape[0] * line, shard.shape[1])
+            if dimension == 0
+            else (shard.shape[0], shard.shape[1] * line),
+            jnp.bfloat16,
+        )
         for shard, dimension in zip(shards, dimensions)
     ]
-    sent = sum(2 * shard.size for shard in shards) * (line - 1)
+    out_specs = [anywhere] * count
+    scratch = []
+    dma = pltpu.SemaphoreType.DMA
+    if count:
+        scratch += [dma((count,))] + [dma((units, 2, line))] * 2
+        scratch += [dma((units, 2, line, max(parts - 1, 1)))] * 2
+    if spread:
+        operands.append(block)
+        shapes.append(jax.ShapeDtypeStruct((block.shape[0], block.shape[1] * ranks), block.dtype))
+        out_specs.append(anywhere)
+        scratch += [dma] + [dma((ranks,))] * 2
+    if summed:
+        operands.append(partial)
+        length, width = partial.shape[0], partial.shape[1] // ranks
+        shapes += [
+            jax.ShapeDtypeStruct((length, width), jnp.float32),
+            jax.ShapeDtypeStruct((length, 128), jnp.float32),
+        ]
+        out_specs += [vmem] * 2
+        scratch += [pltpu.VMEM((ranks // 2, length, width), jnp.bfloat16)] * 3
+        scratch += [pltpu.VMEM((8, length), jnp.float32), pltpu.VMEM((ranks, 8, length), jnp.float32)]
+        scratch += [dma((ranks // 2,))] * 4 + [dma((ranks,))] * 2
     return pl.pallas_call(
-        functools.partial(gather_kernel, dimensions),
-        out_shape=[jax.ShapeDtypeStruct(shape, jnp.bfloat16) for shape in shapes],
-        in_specs=[pl.BlockSpec(memory_space=pltpu.VMEM)] * count,
-        out_specs=[pl.BlockSpec(memory_space=pl.ANY)] * count,
-        scratch_shapes=[
-            pltpu.SemaphoreType.DMA((count,)),
-            pltpu.SemaphoreType.DMA((count, 2, line)),
-            pltpu.SemaphoreType.DMA((count, 2, line)),
-            pltpu.SemaphoreType.DMA((count, 2, line, max(parts - 1, 1))),
-            pltpu.SemaphoreType.DMA((count, 2, line, max(parts - 1, 1))),
-        ],
+        functools.partial(gather_kernel, dimensions, cuts, spread, summed),
+        out_shape=shapes,
+        in_specs=[vmem] * len(operands),
+        out_specs=out_specs,
+        scratch_shapes=scratch,
         compiler_params=pltpu.CompilerParams(collective_id=identity, has_side_effects=True),
-        cost_estimate=pl.CostEstimate(flops=0, bytes_accessed=30 * sent, transcendentals=0),
-    )(*shards)
+    )(*operands)
 
 
 def on_device(
@@ -326,11 +504,13 @@
     length, own_columns = block_source_tensor.shape
     tp_index = lax.axis_index("tp")
     full_width = own_columns * lax.axis_size("tp")
-    full_rows = lax.all_gather(block_source_tensor, "tp", axis=1, tiled=True)
+    question_full, address_full, payload_full, combining_full, full_rows = exchange(
+        (question_map, address_map, payload_weights_map, combining_map),
+        (0, 0, 0, 1),
+        1,
+        block=block_source_tensor,
+    )
     normed = norm_rows(full_rows.astype(jnp.float32), attend_initial_norm_gain).astype(jnp.bfloat16)
-    question_full, address_full, payload_full, combining_full = gather_maps(
-        (question_map, address_map, payload_weights_map, combining_map), (0, 0, 0, 1), 1
-    )
     query, key, value = (
         jnp.dot(normed, full, preferred_element_type=jnp.float32).astype(jnp.bfloat16)
         for full in (question_full, address_full, payload_full)
@@ -351,25 +531,17 @@
         combining_full,
         preferred_element_type=jnp.float32,
     )
-    partials = partials.astype(jnp.bfloat16)
-    valve_shard, partials = lax.optimization_barrier((valve_map, partials))
-    (valve_full,) = gather_maps((valve_shard,), (0,), 2)
-    mixed = lax.psum_scatter(
-        partials, "tp", scatter_dimension=1, tiled=True
-    )
-    mixed, valve_full = lax.optimization_barrier((mixed, valve_full))
-    mixed = mixed.astype(jnp.float32)
-    squares = lax.psum(jnp.sum(mixed * mixed, axis=1), "tp")
+    valve_full, mixed, squares = exchange(
+        (valve_map,), (0,), 2, partial=partials.astype(jnp.bfloat16)
+    )
     own_gain = lax.dynamic_slice_in_dim(attend_final_norm_gain, tp_index * own_columns, own_columns)
     first = (
         block_source_tensor.astype(jnp.float32)
-        + mixed * lax.rsqrt(squares / full_width + epsilon)[:, None] * own_gain
+        + mixed * lax.rsqrt(squares[:, :1] / full_width + epsilon) * own_gain
     ).astype(jnp.bfloat16)
-    widening_shard, narrowing_shard, first = lax.optimization_barrier(
-        (widening_map, narrowing_map, first)
-    )
-    widening_full, narrowing_full = gather_maps((widening_shard, narrowing_shard), (0, 1), 3)
-    first_rows = lax.all_gather(first, "tp", axis=1, tiled=True)
+    widening_full, narrowing_full, first_rows = exchange(
+        (widening_map, narrowing_map), (0, 1), 3, block=first
+    )
     ffn_in = norm_rows(first_rows.astype(jnp.float32), dense_initial_norm_gain).astype(jnp.bfloat16)
 
     gate_pre = jnp.dot(ffn_in, valve_full, preferred_element_type=jnp.float32)
@@ -383,14 +555,11 @@
         narrowing_full,
         preferred_element_type=jnp.float32,
     )
-    channel = lax.psum_scatter(
-        down_partials.astype(jnp.bfloat16), "tp", scatter_dimension=1, tiled=True
-    ).astype(jnp.float32)
-    channel_squares = lax.psum(jnp.sum(channel * channel, axis=1), "tp")
+    channel, channel_squares = exchange((), (), 4, partial=down_partials.astype(jnp.bfloat16))
     own_post = lax.dynamic_slice_in_dim(dense_final_norm_gain, tp_index * own_columns, own_columns)
     return (
         first.astype(jnp.float32)
-        + channel * lax.rsqrt(channel_squares / full_width + epsilon)[:, None] * own_post
+        + channel * lax.rsqrt(channel_squares[:, :1] / full_width + epsilon) * own_post
     ).astype(jnp.bfloat16)
 
 

time: 285 us -> 232 us (0.81)
  waiting for transfers between devices: 29.7 us -> 0 us
  between operations: 13.3 us -> 0.21 us
  blocking collectives: 11.4 us -> 0 us
    reduce_scatter x2 -> x0, waiting for transfers between devices: 28.9 us -> none  [the longest x1 28.9 us: on_device(): lax.psum_scatter(down_partials.astype(jnp.bfloat16), 'tp', scatter_dimens...]
    psum x2 -> x0, blocking collectives: 11.4 us -> none  [the longest x1 5.76 us: on_device(): channel_squares = lax.psum(jnp.sum(channel * channel, axis=1), 'tp')]
    pallas_call x3 -> x4, Pallas kernels: 186 us -> 188 us  [exchange(): pl.pallas_call(functools.partial(gather_kernel, dimensions, cuts, spread,...]
  transfers between devices with their start and end apart: 4 -> 0, of which waited for: 1 -> 0; matrix products, arithmetic and copies ran while one was open for 1% -> 0% of each run, Pallas kernels for 66% -> 0%
where the time goes in v3:
time: 232 us
  Pallas kernels  197 us (85%)
  matrix products  21.8 us (9%)
  other arithmetic  11.2 us (5%)
    pallas_call x4, Pallas kernels, exchange(): pl.pallas_call(functools.partial(gather_kernel, dimensions, cuts, spread,...  188 us
    pallas_call x1, Pallas kernels, mixing(): pl.pallas_call(mixing_kernel, out_shape=jax.ShapeDtypeStruct(value.shape,...  8.86 us
    dot_general x3, matrix products, on_device(): jnp.dot(normed, full, preferred_element_type=jnp.float32)  6.75 us

profile of v3, /device:TPU:0, one launch (start us, length us, event | category | flops | bytes accessed | tf_op | source)
XLA Modules:
  0.0 232.0 jit_solution(18289686334379813703)
XLA Ops:
  0.0 65.3 %shard_map.181 = (bf16[2048,256]{1,0:T(8,128)(2,1)}, bf16[2048,256]{1,0:T(8,128)(2,1)}, bf16[2048,512]{1,0:T(8,128)(2,1)}, bf16[512,2048]{1,0:T(8,128)(2,1)}, bf16[512,2048]{1,0:T(8,128)(2,1)}) custom-call(bf16[512,256]{1,0:T(8,128)(2,1)} %refs_0_.3, bf16[512,256]{1,0:T(8,128)(2,1)} %refs_1_.2, bf16[512,512]{1,0:T(8,128)(2,1)} %refs_2_.1, ...), custom_call_target="tpu_custom_call" | custom-call | tf_op jit(solution)/shard_map/pallas_call | solution.py:473
  65.3 2.2 fusion
  67.6 3.8 %convolution_convert_fusion.2.v_ref = bf16[512,512]{1,0:T(8,128)(2,1)} fusion(bf16[2048,512]{1,0:T(8,128)(2,1)} %get-tuple-element.21, bf16[512,2048]{1,0:T(8,128)(2,1)S(1)} %copy-done.2, f32[2048]{0:T(1024)S(1)} %copy-done.12, f32[512]{0:T(512)S(1)} %add_rsqrt_fusion.1), kind=kOutput, calls=%fused_computation.13 | convolution fusion | flops 1078198272 | bytes 4728832 | tf_op jit(solution)/shard_map/dot_general | solution.py:515
  71.4 1.5 convolution_convert_fusion.3.k_ref
  72.9 1.5 convolution_convert_fusion.4.q_ref
  74.3 1.5 fusion.19.low_ref
  75.8 8.9 %shard_map.182 = bf16[512,512]{1,0:T(8,128)(2,1)} custom-call(bf16[512,256]{1,0:T(8,128)(2,1)} %convolution_convert_fusion.4.q_ref, bf16[512,256]{1,0:T(8,128)(2,1)} %convolution_convert_fusion.3.k_ref, bf16[512,512]{1,0:T(8,128)(2,1)} %convolution_convert_fusion.2.v_ref, f32[512,16]{1,0:T(8,128)} %fusion.19.low_ref, f32[16,256]{1,0:T(8,128)} %right_ref.1, ...), custom_call_target="tpu_custom_call" | custom-call | flops 16106127360 | bytes 2097152 | tf_op jit(solution)/shard_map/pallas_call | solution.py:100
  84.7 3.7 %convolution_convert_fusion.1.refs_1_ = bf16[512,2048]{1,0:T(8,128)(2,1)} fusion(bf16[512,512]{1,0:T(8,128)(2,1)} %shard_map.182, bf16[512,2048]{1,0:T(8,128)(2,1)S(1)} %copy-done.9), kind=kOutput, calls=%fused_computation.11 | convolution fusion | flops 1074790400 | bytes 4718592 | tf_op jit(solution)/shard_map/dot_general | solution.py:529
  88.4 37.2 %shard_map.183 = (bf16[2048,768]{1,0:T(8,128)(2,1)}, f32[512,512]{1,0:T(8,128)}, f32[512,128]{1,0:T(8,128)}) custom-call(bf16[512,768]{1,0:T(8,128)(2,1)} %refs_0_.4, bf16[512,2048]{1,0:T(8,128)(2,1)} %convolution_convert_fusion.1.refs_1_), custom_call_target="tpu_custom_call" | custom-call | tf_op jit(solution)/shard_map/pallas_call | solution.py:473
  125.5 1.1 rsqrt_reduce_fusion.1
  126.7 0.8 dynamic_slice.6
  127.4 2.2 add_convert_fusion.1.refs_2_
  129.7 61.8 %shard_map.184 = (bf16[2048,768]{1,0:T(8,128)(2,1)}, bf16[768,2048]{1,0:T(8,128)(2,1)}, bf16[512,2048]{1,0:T(8,128)(2,1)}) custom-call(bf16[512,768]{1,0:T(8,128)(2,1)} %refs_0_.5, bf16[768,512]{1,0:T(8,128)(2,1)} %refs_1_.3, bf16[512,512]{1,0:T(8,128)(2,1)} %add_convert_fusion.1.refs_2_), custom_call_target="tpu_custom_call" | custom-call | tf_op jit(solution)/shard_map/pallas_call | solution.py:473
  191.5 2.2 fusion.3
  193.7 3.9 %fusion.15 = f32[512,768]{1,0:T(8,128)S(1)} fusion(bf16[2048,768]{1,0:T(8,128)(2,1)} %get-tuple-element.26, bf16[512,2048]{1,0:T(8,128)(2,1)S(1)} %copy-done.3, f32[2048]{0:T(1024)S(1)} %copy-done.13, f32[512]{0:T(512)S(1)} %add_rsqrt_fusion), kind=kOutput, calls=%fused_computation.26 | convolution fusion | flops 1614807040 | bytes 6825984 | tf_op jit(solution)/shard_map/dot_general | solution.py:547
  197.7 0.0 copy-start.5
  197.7 0.0 copy-start.6
  197.7 1.9 fusion.13
  199.6 0.1 slice_reduce_fusion.2
  199.7 4.1 %convolution_convert_fusion.refs_0_ = bf16[512,2048]{1,0:T(8,128)(2,1)} fusion(bf16[768,2048]{1,0:T(8,128)(2,1)S(1)} %copy-done.7, f32[512,768]{1,0:T(8,128)S(1)} %fusion.13, f32[512,768]{1,0:T(8,128)S(1)} %fusion.15, f32[768]{0:T(1024)S(1)} %get-tuple-element.35, f32[768]{0:T(1024)S(1)} %get-tuple-element.36, f32[768]{0:T(1024)S(1)} %get-tuple-element.34, ...), kind=kOutput, calls=%fused_computation.10 | convolution fusion | flops 1617952768 | bytes 8407040 | tf_op jit(solution)/shard_map/dot_general | solution.py:553
  203.8 24.1 %shard_map.185 = (f32[512,512]{1,0:T(8,128)}, f32[512,128]{1,0:T(8,128)}) custom-call(bf16[512,2048]{1,0:T(8,128)(2,1)} %convolution_convert_fusion.refs_0_), custom_call_target="tpu_custom_call" | custom-call | tf_op jit(solution)/shard_map/pallas_call | solution.py:473
  227.9 1.1 rsqrt_reduce_fusion
  229.0 0.8 dynamic_slice.7
  229.8 2.2 add_convert_fusion
  (30 shorter events, 0.1 us)
Async XLA Ops:
  0.0 74.3 %copy-start = (bf16[2048,16]{0,1:T(8,128)(2,1)S(1)}, bf16[2048,16]{0,1:T(8,128)(2,1)}, u32[]{:S(2)}) copy-start(bf16[2048,16]{0,1:T(8,128)(2,1)} %param.28) | copy-start | bytes 196612
  0.0 67.6 %copy-start.12 = (f32[2048]{0:T(1024)S(1)}, f32[2048]{0:T(1024)}, u32[]{:S(2)}) copy-start(f32[2048]{0:T(1024)} %param.20) | copy-start | bytes 24580
  65.3 2.3 copy-start.2
  67.6 3.8 %copy-start.11 = (bf16[2048,256]{1,0:T(8,128)(2,1)S(1)}, bf16[2048,256]{1,0:T(8,128)(2,1)}, u32[]{:S(2)}) copy-start(bf16[2048,256]{1,0:T(8,128)(2,1)} %get-tuple-element.20) | copy-start | bytes 3145732
  71.4 1.5 copy-start.10
  75.8 8.9 %copy-start.9 = (bf16[512,2048]{1,0:T(8,128)(2,1)S(1)}, bf16[512,2048]{1,0:T(8,128)(2,1)}, u32[]{:S(2)}) copy-start(bf16[512,2048]{1,0:T(8,128)(2,1)} %get-tuple-element.22) | copy-start | bytes 6291460
  88.4 39.0 %copy-start.4 = (bf16[512,512]{1,0:T(8,128)(2,1)S(1)}, bf16[512,512]{1,0:T(8,128)(2,1)}, u32[]{:S(2)}) copy-start(bf16[512,512]{1,0:T(8,128)(2,1)} %refs_4_.1) | copy-start | bytes 1572868
  129.7 64.1 %copy-start.13 = (f32[2048]{0:T(1024)S(1)}, f32[2048]{0:T(1024)}, u32[]{:S(2)}) copy-start(f32[2048]{0:T(1024)} %param.23) | copy-start | bytes 24580
  191.5 2.3 copy-start.3
  193.7 3.9 %copy-start.8 = (bf16[2048,768]{1,0:T(8,128)(2,1)S(1)}, bf16[2048,768]{1,0:T(8,128)(2,1)}, u32[]{:S(2)}) copy-start(bf16[2048,768]{1,0:T(8,128)(2,1)} %get-tuple-element.27) | copy-start | bytes 9437188
  197.7 1.9 copy-start.5
  197.7 1.9 copy-start.6
  197.7 2.0 copy-start.7
  203.8 26.0 %copy-start.1 = (bf16[512,512]{1,0:T(8,128)(2,1)S(1)}, bf16[512,512]{1,0:T(8,128)(2,1)}, u32[]{:S(2)}) copy-start(bf16[512,512]{1,0:T(8,128)(2,1)} %add_convert_fusion.1.refs_2_) | copy-start | bytes 1572868

commit v4 on v3

--- a/solution.py
+++ b/solution.py
@@ -437,7 +437,7 @@
     cuts = [cuts_of(shard) for shard in shards]
     units = sum(cuts)
     spread, summed = int(block is not None), int(partial is not None)
-    vmem, anywhere = pl.BlockSpec(memory_space=pltpu.VMEM), pl.BlockSpec(memory_space=pl.ANY)
+    vmem = pl.BlockSpec(memory_space=pltpu.VMEM)
     operands = list(shards)
     shapes = [
         jax.ShapeDtypeStruct(
@@ -448,7 +448,7 @@
         )
         for shard, dimension in zip(shards, dimensions)
     ]
-    out_specs = [anywhere] * count
+    out_specs = [vmem] * count
     scratch = []
     dma = pltpu.SemaphoreType.DMA
     if count:
@@ -457,7 +457,7 @@
     if spread:
         operands.append(block)
         shapes.append(jax.ShapeDtypeStruct((block.shape[0], block.shape[1] * ranks), block.dtype))
-        out_specs.append(anywhere)
+        out_specs.append(vmem)
         scratch += [dma] + [dma((ranks,))] * 2
     if summed:
         operands.append(partial)

time: 232 us -> 239 us (1.030)
  Pallas kernels: 197 us -> 204 us
    pallas_call x4, Pallas kernels: 188 us -> 195 us  [exchange(): pl.pallas_call(functools.partial(gather_kernel, dimensions, cuts, spread,...]
where the time goes in v4:
time: 239 us
  Pallas kernels  204 us (85%)
  matrix products  21.8 us (9%)
  other arithmetic  11.2 us (5%)
    pallas_call x4, Pallas kernels, exchange(): pl.pallas_call(functools.partial(gather_kernel, dimensions, cuts, spread,...  195 us
    pallas_call x1, Pallas kernels, mixing(): pl.pallas_call(mixing_kernel, out_shape=jax.ShapeDtypeStruct(value.shape,...  8.86 us
    dot_general x3, matrix products, on_device(): jnp.dot(normed, full, preferred_element_type=jnp.float32)  6.75 us

profile of v4, /device:TPU:0, one launch (start us, length us, event | category | flops | bytes accessed | tf_op | source)
XLA Modules:
  0.0 238.6 jit_solution(8016172711888084415)
XLA Ops:
  0.0 68.2 %shard_map.181 = (bf16[2048,256]{1,0:T(8,128)(2,1)}, bf16[2048,256]{1,0:T(8,128)(2,1)}, bf16[2048,512]{1,0:T(8,128)(2,1)}, bf16[512,2048]{1,0:T(8,128)(2,1)}, bf16[512,2048]{1,0:T(8,128)(2,1)}) custom-call(bf16[512,256]{1,0:T(8,128)(2,1)} %refs_0_.3, bf16[512,256]{1,0:T(8,128)(2,1)} %refs_1_.2, bf16[512,512]{1,0:T(8,128)(2,1)} %refs_2_.1, ...), custom_call_target="tpu_custom_call" | custom-call | tf_op jit(solution)/shard_map/pallas_call | solution.py:473
  68.2 2.2 fusion
  70.4 3.8 %convolution_convert_fusion.2.v_ref = bf16[512,512]{1,0:T(8,128)(2,1)} fusion(bf16[2048,512]{1,0:T(8,128)(2,1)} %get-tuple-element.21, bf16[512,2048]{1,0:T(8,128)(2,1)S(1)} %copy-done.2, f32[2048]{0:T(1024)S(1)} %copy-done.12, f32[512]{0:T(512)S(1)} %add_rsqrt_fusion.1), kind=kOutput, calls=%fused_computation.13 | convolution fusion | flops 1078198272 | bytes 4728832 | tf_op jit(solution)/shard_map/dot_general | solution.py:515
  74.2 1.5 convolution_convert_fusion.3.k_ref
  75.7 1.5 convolution_convert_fusion.4.q_ref
  77.2 1.5 fusion.19.low_ref
  78.7 8.9 %shard_map.182 = bf16[512,512]{1,0:T(8,128)(2,1)} custom-call(bf16[512,256]{1,0:T(8,128)(2,1)} %convolution_convert_fusion.4.q_ref, bf16[512,256]{1,0:T(8,128)(2,1)} %convolution_convert_fusion.3.k_ref, bf16[512,512]{1,0:T(8,128)(2,1)} %convolution_convert_fusion.2.v_ref, f32[512,16]{1,0:T(8,128)} %fusion.19.low_ref, f32[16,256]{1,0:T(8,128)} %right_ref.1, ...), custom_call_target="tpu_custom_call" | custom-call | flops 16106127360 | bytes 2097152 | tf_op jit(solution)/shard_map/pallas_call | solution.py:100
  87.6 3.7 %convolution_convert_fusion.1.refs_1_ = bf16[512,2048]{1,0:T(8,128)(2,1)} fusion(bf16[512,512]{1,0:T(8,128)(2,1)} %shard_map.182, bf16[512,2048]{1,0:T(8,128)(2,1)S(1)} %copy-done.9), kind=kOutput, calls=%fused_computation.11 | convolution fusion | flops 1074790400 | bytes 4718592 | tf_op jit(solution)/shard_map/dot_general | solution.py:529
  91.2 38.0 %shard_map.183 = (bf16[2048,768]{1,0:T(8,128)(2,1)}, f32[512,512]{1,0:T(8,128)}, f32[512,128]{1,0:T(8,128)}) custom-call(bf16[512,768]{1,0:T(8,128)(2,1)} %refs_0_.4, bf16[512,2048]{1,0:T(8,128)(2,1)} %convolution_convert_fusion.1.refs_1_), custom_call_target="tpu_custom_call" | custom-call | tf_op jit(solution)/shard_map/pallas_call | solution.py:473
  129.2 1.1 rsqrt_reduce_fusion.1
  130.3 0.8 dynamic_slice.6
  131.1 2.2 add_convert_fusion.1.refs_2_
  133.3 64.7 %shard_map.184 = (bf16[2048,768]{1,0:T(8,128)(2,1)}, bf16[768,2048]{1,0:T(8,128)(2,1)}, bf16[512,2048]{1,0:T(8,128)(2,1)}) custom-call(bf16[512,768]{1,0:T(8,128)(2,1)} %refs_0_.5, bf16[768,512]{1,0:T(8,128)(2,1)} %refs_1_.3, bf16[512,512]{1,0:T(8,128)(2,1)} %add_convert_fusion.1.refs_2_), custom_call_target="tpu_custom_call" | custom-call | tf_op jit(solution)/shard_map/pallas_call | solution.py:473
  198.0 2.2 fusion.3
  200.3 3.9 %fusion.15 = f32[512,768]{1,0:T(8,128)S(1)} fusion(bf16[2048,768]{1,0:T(8,128)(2,1)} %get-tuple-element.26, bf16[512,2048]{1,0:T(8,128)(2,1)S(1)} %copy-done.3, f32[2048]{0:T(1024)S(1)} %copy-done.13, f32[512]{0:T(512)S(1)} %add_rsqrt_fusion), kind=kOutput, calls=%fused_computation.26 | convolution fusion | flops 1614807040 | bytes 6825984 | tf_op jit(solution)/shard_map/dot_general | solution.py:547
  204.2 0.0 copy-start.5
  204.3 0.0 copy-start.6
  204.3 1.9 fusion.13
  206.2 0.1 slice_reduce_fusion.2
  206.3 4.1 %convolution_convert_fusion.refs_0_ = bf16[512,2048]{1,0:T(8,128)(2,1)} fusion(bf16[768,2048]{1,0:T(8,128)(2,1)S(1)} %copy-done.7, f32[512,768]{1,0:T(8,128)S(1)} %fusion.13, f32[512,768]{1,0:T(8,128)S(1)} %fusion.15, f32[768]{0:T(1024)S(1)} %get-tuple-element.35, f32[768]{0:T(1024)S(1)} %get-tuple-element.36, f32[768]{0:T(1024)S(1)} %get-tuple-element.34, ...), kind=kOutput, calls=%fused_computation.10 | convolution fusion | flops 1617952768 | bytes 8407040 | tf_op jit(solution)/shard_map/dot_general | solution.py:553
  210.3 24.1 %shard_map.185 = (f32[512,512]{1,0:T(8,128)}, f32[512,128]{1,0:T(8,128)}) custom-call(bf16[512,2048]{1,0:T(8,128)(2,1)} %convolution_convert_fusion.refs_0_), custom_call_target="tpu_custom_call" | custom-call | tf_op jit(solution)/shard_map/pallas_call | solution.py:473
  234.4 1.1 rsqrt_reduce_fusion
  235.6 0.8 dynamic_slice.7
  236.3 2.2 add_convert_fusion
  (30 shorter events, 0.1 us)
Async XLA Ops:
  0.0 77.2 %copy-start = (bf16[2048,16]{0,1:T(8,128)(2,1)S(1)}, bf16[2048,16]{0,1:T(8,128)(2,1)}, u32[]{:S(2)}) copy-start(bf16[2048,16]{0,1:T(8,128)(2,1)} %param.28) | copy-start | bytes 196612
  0.0 70.4 %copy-start.12 = (f32[2048]{0:T(1024)S(1)}, f32[2048]{0:T(1024)}, u32[]{:S(2)}) copy-start(f32[2048]{0:T(1024)} %param.20) | copy-start | bytes 24580
  68.2 2.3 copy-start.2
  70.4 3.8 %copy-start.11 = (bf16[2048,256]{1,0:T(8,128)(2,1)S(1)}, bf16[2048,256]{1,0:T(8,128)(2,1)}, u32[]{:S(2)}) copy-start(bf16[2048,256]{1,0:T(8,128)(2,1)} %get-tuple-element.20) | copy-start | bytes 3145732
  74.2 1.5 copy-start.10
  78.7 8.9 %copy-start.9 = (bf16[512,2048]{1,0:T(8,128)(2,1)S(1)}, bf16[512,2048]{1,0:T(8,128)(2,1)}, u32[]{:S(2)}) copy-start(bf16[512,2048]{1,0:T(8,128)(2,1)} %get-tuple-element.22) | copy-start | bytes 6291460
  91.2 39.9 %copy-start.4 = (bf16[512,512]{1,0:T(8,128)(2,1)S(1)}, bf16[512,512]{1,0:T(8,128)(2,1)}, u32[]{:S(2)}) copy-start(bf16[512,512]{1,0:T(8,128)(2,1)} %refs_4_.1) | copy-start | bytes 1572868
  133.3 66.9 %copy-start.13 = (f32[2048]{0:T(1024)S(1)}, f32[2048]{0:T(1024)}, u32[]{:S(2)}) copy-start(f32[2048]{0:T(1024)} %param.23) | copy-start | bytes 24580
  198.0 2.3 copy-start.3
  200.3 3.9 %copy-start.8 = (bf16[2048,768]{1,0:T(8,128)(2,1)S(1)}, bf16[2048,768]{1,0:T(8,128)(2,1)}, u32[]{:S(2)}) copy-start(bf16[2048,768]{1,0:T(8,128)(2,1)} %get-tuple-element.27) | copy-start | bytes 9437188
  204.2 1.9 copy-start.5
  204.3 1.9 copy-start.6
  204.3 2.0 copy-start.7
  210.3 26.0 %copy-start.1 = (bf16[512,512]{1,0:T(8,128)(2,1)S(1)}, bf16[512,512]{1,0:T(8,128)(2,1)}, u32[]{:S(2)}) copy-start(bf16[512,512]{1,0:T(8,128)(2,1)} %add_convert_fusion.1.refs_2_) | copy-start | bytes 1572868
